TPU v7x, 512 devices: a whole 4x8x8 slice. The times are simulated.
512 devices in a mesh: sp: 32 (over z, x), tp: 16 (over y, core).
Axes of the slice: x: 4, y: 8, z: 8, core: 2. Of those that a mesh axis runs over, the one named last changes fastest.
Arguments:
- stream_in: bfloat16 [8192, 2048], P(('sp', 'tp')), may hold values from -6 to 6
- pre_gate: bfloat16 [8192, 1024], P('sp', 'tp'), may hold values from -6 to 6
- value_in: bfloat16 [8192, 1024], P('sp', 'tp'), may hold values from -6 to 6
- post_gate: bfloat16 [8192, 1024], P('sp', 'tp'), may hold values from -6 to 6
- conv_taps: bfloat16 [3, 1024], P(None, 'tp'), may hold values from -3 to 3
- out_weight: bfloat16 [1024, 2048], P('tp'), may hold values from -0.1875 to 0.1875
- route_ids: int32 [8192, 4], P('sp'), may hold values from 0 to 31, all different within a row; in each aligned block of 16 rows (0 to 15, 16 to 31, ...) at most 4 rows name the same one
- route_weight: float32 [8192, 4], P('sp'), may hold values from 0.1 to 1
- ffn_gain: bfloat16 [2048], replicated, may hold values from 0.099609375 to 1.8984375
- post_gain: bfloat16 [2048], replicated, may hold values from 0.099609375 to 1.8984375
- gate_proj: bfloat16 [32, 2048, 2048], P('sp', None, 'tp'), may hold values from -0.39648438 to 0.39648438
- up_proj: bfloat16 [32, 2048, 2048], P('sp', None, 'tp'), may hold values from -0.39648438 to 0.39648438
- down_proj: bfloat16 [32, 2048, 2048], P('sp', None, 'tp'), may hold values from -0.125 to 0.125
Outputs:
- layer_out: bfloat16 [8192, 2048], P(('sp', 'tp'))
Inputs may be any that keep to these rules, and one draw needn't show every extreme that they name: `route_ids`: in each aligned block of 16 positions, a row names 4 different experts and no expert is named by more than 4 rows; in every draw some expert reaches 4 in some block.
All inputs are finite; a program needn't handle non-finite values.
Results may differ from a plain program's by a relative error of at most 0.014.
Values may be sent and summed in bfloat16 or wider, within the bound.
A program may use at most 64 MiB of HBM per device.

v0:
```python
import jax
import jax.numpy as jnp
from jax import lax
from jax.sharding import PartitionSpec as P

clamp_limit = 7.0
sigmoid_scale = 1.702
epsilon = 1e-06


def passed_along(array, axis, by):
    count = lax.axis_size(axis)
    pairs = [(i, i + by) for i in range(count) if 0 <= i + by < count]
    return lax.ppermute(array, axis, pairs)


def clamped_units(gate_pre, up_pre):
    gate_cut = jnp.minimum(gate_pre, clamp_limit)
    up_cut = jnp.clip(up_pre, -clamp_limit, clamp_limit)
    return (up_cut + 1.0) * (gate_cut * jax.nn.sigmoid(sigmoid_scale * gate_cut))


def scaled_norm(values, gain):
    return (
        values
        * lax.rsqrt(jnp.mean(values * values, axis=-1, keepdims=True) + epsilon)
        * gain.astype(jnp.float32)
    )


def block_ranks(route_rows, experts, block_rows):
    flattened = route_rows.reshape(-1)
    entries = flattened.shape[0]
    span_width = block_rows * route_rows.shape[1]
    onehot = (flattened[:, None] == jnp.arange(experts, dtype=jnp.int32)[None, :]).astype(jnp.int32)
    blocked = onehot.reshape(entries // span_width, span_width, experts)
    before = jnp.cumsum(blocked, axis=1) - blocked
    return jnp.sum(before * blocked, axis=2).reshape(route_rows.shape)


def slot_picker(slot_index, table_size):
    matches = slot_index[None, :, :] == jnp.arange(table_size, dtype=jnp.int32)[:, None, None]
    return jnp.any(matches, axis=2).astype(jnp.bfloat16)


def local(
    stream_in,
    pre_gate,
    value_in,
    post_gate,
    conv_taps,
    out_weight,
    route_ids,
    route_weight,
    ffn_gain,
    post_gain,
    gate_proj,
    up_proj,
    down_proj,
):
    sp_count = lax.axis_size("sp")
    tp_count = lax.axis_size("tp")
    seq_rows = pre_gate.shape[0]
    own_rows = seq_rows // tp_count
    top_count = route_ids.shape[1]
    slots_each = 2 * own_rows * top_count // sp_count
    tap_count = conv_taps.shape[0]
    gated_input = (pre_gate.astype(jnp.float32) * value_in.astype(jnp.float32)).astype(jnp.bfloat16)
    rim_rows = passed_along(gated_input[seq_rows - tap_count + 1 :], "sp", 1)
    padded = jnp.concatenate([rim_rows, gated_input], 0).astype(jnp.float32)
    convolved = jnp.zeros(gated_input.shape, jnp.float32)
    for tap_index in range(tap_count):
        convolved = (
            convolved
            + conv_taps[tap_index].astype(jnp.float32)[None, :]
            * padded[tap_index : tap_index + seq_rows]
        )
    mixer_out = (post_gate.astype(jnp.float32) * convolved).astype(jnp.bfloat16)
    spread = lax.all_to_all(mixer_out, "tp", split_axis=0, concat_axis=1, tiled=True)
    projected = jnp.dot(
        spread,
        lax.all_gather(out_weight, "tp", axis=0, tiled=True),
        preferred_element_type=jnp.float32,
    )
    residual = (stream_in.astype(jnp.float32) + projected).astype(jnp.bfloat16)
    normed = scaled_norm(residual.astype(jnp.float32), ffn_gain).astype(jnp.bfloat16)
    slot_rank = block_ranks(route_ids, sp_count, own_rows)
    block_of = (jnp.arange(seq_rows, dtype=jnp.int32) // own_rows)[:, None]
    tp_index = lax.axis_index("tp")
    own_ids = lax.dynamic_slice_in_dim(route_ids, tp_index * own_rows, own_rows, 0)
    own_rank = lax.dynamic_slice_in_dim(slot_rank, tp_index * own_rows, own_rows, 0)
    own_slot = own_ids * slots_each + own_rank
    picker = slot_picker(own_slot, sp_count * slots_each)
    outgoing = jnp.dot(picker, normed, preferred_element_type=jnp.float32).astype(jnp.bfloat16)
    arrived = lax.all_to_all(outgoing, "sp", split_axis=0, concat_axis=0, tiled=True)
    portion = lax.all_gather(arrived, "tp", axis=0, tiled=True)
    gate_pre = jnp.dot(portion, gate_proj[0], preferred_element_type=jnp.float32)
    up_pre = jnp.dot(portion, up_proj[0], preferred_element_type=jnp.float32)
    hidden = clamped_units(gate_pre, up_pre).astype(jnp.bfloat16)
    weight_rows = down_proj[0]
    column_out = jnp.dot(
        lax.all_gather(hidden, "tp", axis=1, tiled=True),
        weight_rows,
        preferred_element_type=jnp.float32,
    ).astype(jnp.bfloat16)
    column_width = column_out.shape[1]
    returned = lax.all_to_all(
        column_out.reshape(tp_count, sp_count, slots_each, column_width),
        "sp",
        split_axis=1,
        concat_axis=1,
        tiled=True,
    )
    home_index = (block_of * sp_count + route_ids) * slots_each + slot_rank
    gathered_out = jnp.take(returned.reshape(-1, column_width), home_index.reshape(-1), axis=0)
    gathered_out = gathered_out.astype(jnp.float32).reshape(seq_rows, top_count, column_width)
    combined_cols = jnp.sum(gathered_out * route_weight[:, :, None], axis=1).astype(jnp.bfloat16)
    combined = lax.all_to_all(combined_cols, "tp", split_axis=0, concat_axis=1, tiled=True)
    layer_out = residual.astype(jnp.float32) + scaled_norm(combined.astype(jnp.float32), post_gain)
    return layer_out.astype(jnp.bfloat16)


def solution(mesh):
    placed = (
        P(("sp", "tp"), None),
        P("sp", "tp"),
        P("sp", "tp"),
        P("sp", "tp"),
        P(None, "tp"),
        P("tp", None),
        P("sp", None),
        P("sp", None),
        P(),
        P(),
        P("sp", None, "tp"),
        P("sp", None, "tp"),
        P("sp", None, "tp"),
    )
    return jax.shard_map(
        local, mesh=mesh, in_specs=placed, out_specs=P(("sp", "tp"), None), check_vma=False
    )
```

profile of v0, /device:TPU:1, one launch (start us, length us, event | category | flops | bytes accessed | tf_op | source)
XLA Modules:
  0.0 280.2 jit_solution(12051005114207174218)
XLA Ops:
  6.5 0.7 all-gather.4.cloned.1.call-update
  7.3 0.8 multiply_convert_fusion.2
  8.1 3.9 %collective-permute-start = (bf16[2,64]{0,1:T(8,128)(2,1)S(1)}, bf16[2,64]{0,1:T(8,128)(2,1)S(1)}, u32[]{:S(2)}, u32[]{:S(2)}) collective-permute-start(bf16[2,64]{0,1:T(8,128)(2,1)S(1)} %slice.30), channel_id=1, source_target_pairs={{0,16},{16,32},{32,48},{48,64},{64,80},{80,96},{96,112},{112,128},... | collective-permute-start | bytes 776 | tf_op jit(solution)/shard_map/ppermute | solution.py:14
  12.1 0.8 copy.62
  13.1 1.4 select_reduce_fusion
  14.7 0.8 bitcast_convert_fusion.2
  15.6 0.7 convert_element_type.94
  16.4 0.9 fusion.19
  17.4 0.7 reshape.125
  18.1 8.1 %all-to-all-start = ((bf16[16,2,512]{2,1,0:T(2,128)(2,1)}), bf16[16,2,512]{2,1,0:T(2,128)(2,1)S(1)}, u32[]{:S(2)}, u32[]{:S(2)}) async-start(bf16[16,2,512]{2,1,0:T(2,128)(2,1)} %reshape.125), calls=%async_computation | async-start | bytes 65536 | tf_op jit(solution)/shard_map/all_to_all | solution.py:79
  26.3 7.3 %all-to-all-done = bf16[16,2,512]{2,1,0:T(2,128)(2,1)S(1)} async-done(((bf16[16,2,512]{2,1,0:T(2,128)(2,1)}), bf16[16,2,512]{2,1,0:T(2,128)(2,1)S(1)}, u32[]{:S(2)}, u32[]{:S(2)}) %all-to-all-start) | async-done | bytes 32800 | tf_op jit(solution)/shard_map/all_to_all | solution.py:79
  33.8 25.8 %all-gather.4.cloned.1.call-done = bf16[1024,2048]{1,0:T(8,128)(2,1)} async-done(((bf16[64,2048]{1,0:T(8,128)(2,1)}), bf16[1024,2048]{1,0:T(8,128)(2,1)}) %all-gather.4.cloned.1.call-update) | async-done | bytes 4194320 | tf_op jit(solution)/shard_map/all_gather | solution.py:82
  59.7 3.0 %multiply_reduce_fusion.1 = (f32[16]{0:T(128)S(1)}, f32[16,2048]{1,0:T(8,128)S(1)}) fusion(bf16[16,1024]{1,0:T(8,128)(2,1)S(1)} %all_to_all.36, bf16[1024,2048]{1,0:T(8,128)(2,1)} %all-gather.4.cloned.1.call-done, bf16[16,2048]{1,0:T(8,128)(2,1)} %param.13), kind=kOutput, calls=%fused_computation.29 | convolution fusion | flops 67305456 | bytes 4423744 | tf_op jit(solution)/shard_map/dot_general | solution.py:80
  62.7 0.3 convolution_convert_fusion.1
  63.0 0.2 all_to_all.37
  63.2 26.7 %all_to_all.46 = bf16[32,4,2048]{2,1,0:T(4,128)(2,1)S(1)} all-to-all(bf16[32,4,2048]{2,1,0:T(4,128)(2,1)S(1)} %all_to_all.37), channel_id=1, replica_groups=mesh['sp'=32,'tp'=16] {'sp'}, dimensions={0} | all-to-all | bytes 1048576 | tf_op jit(solution)/shard_map/all_to_all | solution.py:95
  89.9 1.0 all_to_all.39
  90.9 53.9 %all-gather.6.cloned.1.call-done = bf16[2048,2048]{1,0:T(8,128)(2,1)} async-done(((bf16[128,2048]{1,0:T(8,128)(2,1)}), bf16[2048,2048]{1,0:T(8,128)(2,1)}) %all-gather.6.cloned.1.call-update) | async-done | bytes 8388624 | tf_op jit(solution)/shard_map/all_gather | solution.py:96
  144.8 5.9 %convolution_minimum_fusion = f32[2048,128]{1,0:T(8,128)S(1)} fusion(bf16[2048,2048]{1,0:T(8,128)(2,1)} %all-gather.6.cloned.1.call-done, bf16[1,2048,128]{2,1,0:T(8,128)(2,1)S(1)} %copy-done), kind=kOutput, calls=%fused_computation.1 | convolution fusion | flops 1074003968 | bytes 9961472 | tf_op jit(solution)/shard_map/dot_general | solution.py:97
  150.8 3.3 %fusion.2 = bf16[2048,128]{1,0:T(8,128)(2,1)} fusion(bf16[2048,2048]{1,0:T(8,128)(2,1)S(1)} %copy-done.4, f32[2048,128]{1,0:T(8,128)S(1)} %convolution_minimum_fusion, bf16[1,2048,128]{2,1,0:T(8,128)(2,1)S(1)} %copy-done.5), kind=kOutput, calls=%fused_computation.5 | convolution fusion | flops 1076101120 | bytes 10485760 | tf_op jit(solution)/shard_map/dot_general | solution.py:98
  154.1 68.6 %all-gather.8.cloned.1.call-done = bf16[2048,2048]{1,0:T(8,128)(2,1)} async-done(((bf16[2048,128]{1,0:T(8,128)(2,1)}), bf16[2048,2048]{1,0:T(8,128)(2,1)}) %all-gather.8.cloned.1.call-update) | async-done | bytes 8388624 | tf_op jit(solution)/shard_map/all_gather | solution.py:102
  222.8 5.7 %convolution_convert_fusion = bf16[2048,128]{1,0:T(8,128)(2,1)S(1)} fusion(bf16[2048,2048]{1,0:T(8,128)(2,1)} %all-gather.8.cloned.1.call-done, bf16[1,2048,128]{2,1,0:T(8,128)(2,1)S(1)} %copy-done.6), kind=kOutput, calls=%fused_computation.6 | convolution fusion | flops 1074003968 | bytes 9437184 | tf_op jit(solution)/shard_map/dot_general | solution.py:101
  228.5 1.1 copy.69
  229.6 6.9 %all-to-all-start.2 = ((bf16[16,32,4,128]{3,2,0,1:T(4,128)(2,1)}), bf16[16,32,4,128]{3,2,0,1:T(4,128)(2,1)S(1)}, u32[]{:S(2)}, u32[]{:S(2)}) async-start(bf16[16,32,4,128]{3,2,0,1:T(4,128)(2,1)} %copy.69), calls=%async_computation.2 | async-start | bytes 1048576 | tf_op jit(solution)/shard_map/all_to_all | solution.py:107
  236.9 0.2 copy.66
  237.2 15.9 %all-to-all-done.2 = bf16[16,32,4,128]{3,2,0,1:T(4,128)(2,1)S(1)} async-done(((bf16[16,32,4,128]{3,2,0,1:T(4,128)(2,1)}), bf16[16,32,4,128]{3,2,0,1:T(4,128)(2,1)S(1)}, u32[]{:S(2)}, u32[]{:S(2)}) %all-to-all-start.2) | async-done | bytes 524320 | tf_op jit(solution)/shard_map/all_to_all | solution.py:107
  253.1 0.2 copy.70
  253.3 3.2 %gather_fusion = bf16[1024,128]{1,0:T(8,128)(2,1)S(1)} fusion(bf16[2048,128]{1,0:T(8,128)(2,1)S(1)} %bitcast.43, s32[1024]{0:T(1024)S(1)} %broadcast_clamp_fusion), kind=kCustom, calls=%fused_computation | custom fusion | bytes 528384 | tf_op jit(solution)/shard_map/jit(_take)/gather | solution.py:115
  256.5 2.1 multiply_reduce_fusion
  258.6 6.4 %all-to-all-start.3 = ((bf16[16,16,128]{2,1,0:T(8,128)(2,1)}), bf16[16,16,128]{2,1,0:T(8,128)(2,1)S(1)}, u32[]{:S(2)}, u32[]{:S(2)}) async-start(bf16[16,16,128]{2,1,0:T(8,128)(2,1)} %bitcast.12), calls=%async_computation.3 | async-start | bytes 131072 | tf_op jit(solution)/shard_map/all_to_all | solution.py:118
  265.0 7.8 %all-to-all-done.3 = bf16[16,16,128]{2,1,0:T(8,128)(2,1)S(1)} async-done(((bf16[16,16,128]{2,1,0:T(8,128)(2,1)}), bf16[16,16,128]{2,1,0:T(8,128)(2,1)S(1)}, u32[]{:S(2)}, u32[]{:S(2)}) %all-to-all-start.3) | async-done | bytes 65568 | tf_op jit(solution)/shard_map/all_to_all | solution.py:118
  272.9 0.7 fusion.16
  (45 shorter events, 1.8 us)
Async XLA Ops:
  6.5 138.3 %copy-start = (bf16[1,2048,128]{2,1,0:T(8,128)(2,1)S(1)}, bf16[1,2048,128]{2,1,0:T(8,128)(2,1)}, u32[]{:S(2)}) copy-start(bf16[1,2048,128]{2,1,0:T(8,128)(2,1)} %param.23) | copy-start | bytes 1572868
  6.5 53.1 %all-gather.4.cloned.1.call-start = ((), (), s32[]{:S(2)}) async-start(), calls=%async_computation.4 | async-start | bytes 4456448 | tf_op jit(solution)/shard_map/all_gather | solution.py:82
  8.1 8.2 %collective-permute-start = (bf16[2,64]{0,1:T(8,128)(2,1)S(1)}, bf16[2,64]{0,1:T(8,128)(2,1)S(1)}, u32[]{:S(2)}, u32[]{:S(2)}) collective-permute-start(bf16[2,64]{0,1:T(8,128)(2,1)S(1)} %slice.30), channel_id=1, source_target_pairs={{0,16},{16,32},{32,48},{48,64},{64,80},{80,96},{96,112},{112,128},... | collective-permute-start | bytes 776 | tf_op jit(solution)/shard_map/ppermute | solution.py:14
  18.1 15.5 %all-to-all-start = ((bf16[16,2,512]{2,1,0:T(2,128)(2,1)}), bf16[16,2,512]{2,1,0:T(2,128)(2,1)S(1)}, u32[]{:S(2)}, u32[]{:S(2)}) async-start(bf16[16,2,512]{2,1,0:T(2,128)(2,1)} %reshape.125), calls=%async_computation | async-start | bytes 65536 | tf_op jit(solution)/shard_map/all_to_all | solution.py:79
  26.2 118.6 %all-gather.6.cloned.1.call-start = ((), (), s32[]{:S(2)}) async-start(), calls=%async_computation.5 | async-start | bytes 8912896 | tf_op jit(solution)/shard_map/all_gather | solution.py:96
  62.6 88.1 %copy-start.5 = (bf16[1,2048,128]{2,1,0:T(8,128)(2,1)S(1)}, bf16[1,2048,128]{2,1,0:T(8,128)(2,1)}, u32[]{:S(2)}) copy-start(bf16[1,2048,128]{2,1,0:T(8,128)(2,1)} %param.24) | copy-start | bytes 1572868
  90.9 131.9 %all-gather.8.cloned.1.call-start = ((), (), s32[]{:S(2)}) async-start(), calls=%async_computation.6 | async-start | bytes 8912896 | tf_op jit(solution)/shard_map/all_gather | solution.py:102
  144.8 5.9 %copy-start.4 = (bf16[2048,2048]{1,0:T(8,128)(2,1)S(1)}, bf16[2048,2048]{1,0:T(8,128)(2,1)}, u32[]{:S(2)}) copy-start(bf16[2048,2048]{1,0:T(8,128)(2,1)} %all-gather.6.cloned.1.call-done) | copy-start | bytes 25165828
  150.8 72.0 %copy-start.6 = (bf16[1,2048,128]{2,1,0:T(8,128)(2,1)S(1)}, bf16[1,2048,128]{2,1,0:T(8,128)(2,1)}, u32[]{:S(2)}) copy-start(bf16[1,2048,128]{2,1,0:T(8,128)(2,1)} %param.25) | copy-start | bytes 1572868
  154.1 82.5 %copy-start.1 = (s32[256,4]{0,1:T(4,128)S(1)}, s32[256,4]{0,1:T(4,128)}, u32[]{:S(2)}) copy-start(s32[256,4]{0,1:T(4,128)} %param.19) | copy-start | bytes 12292
  154.1 83.0 %copy-start.2 = (f32[256,4]{0,1:T(4,128)S(1)}, f32[256,4]{0,1:T(4,128)}, u32[]{:S(2)}) copy-start(f32[256,4]{0,1:T(4,128)} %param.20) | copy-start | bytes 12292
  154.1 110.9 %copy-start.3 = (bf16[2048]{0:T(1024)(128)(2,1)S(1)}, bf16[2048]{0:T(1024)(128)(2,1)}, u32[]{:S(2)}) copy-start(bf16[2048]{0:T(1024)(128)(2,1)} %param.22) | copy-start | bytes 12292
  229.6 23.5 %all-to-all-start.2 = ((bf16[16,32,4,128]{3,2,0,1:T(4,128)(2,1)}), bf16[16,32,4,128]{3,2,0,1:T(4,128)(2,1)S(1)}, u32[]{:S(2)}, u32[]{:S(2)}) async-start(bf16[16,32,4,128]{3,2,0,1:T(4,128)(2,1)} %copy.69), calls=%async_computation.2 | async-start | bytes 1048576 | tf_op jit(solution)/shard_map/all_to_all | solution.py:107
  258.6 14.2 %all-to-all-start.3 = ((bf16[16,16,128]{2,1,0:T(8,128)(2,1)}), bf16[16,16,128]{2,1,0:T(8,128)(2,1)S(1)}, u32[]{:S(2)}, u32[]{:S(2)}) async-start(bf16[16,16,128]{2,1,0:T(8,128)(2,1)} %bitcast.12), calls=%async_computation.3 | async-start | bytes 131072 | tf_op jit(solution)/shard_map/all_to_all | solution.py:118
Sparse Core Ops, SparseCore 0:
  9.5 50.1 all-gather.3
  91.0 53.7 all-gather.5
  154.2 68.4 all-gather.7
where the time goes:
time: 281 us; the launch traced here: 280 us
  waiting for transfers between devices  180 us (64%)
  blocking collectives  26.7 us (10%)
  starting transfers between devices  25.4 us (9%)
  matrix products  18.2 us (6%)
  between operations  13.4 us (5%)
  local copies, waits for them, and re-layouts  8.78 us (3%)
  other arithmetic  7.76 us (3%)
    all_gather x1, waiting for transfers between devices, local(): lax.all_gather(hidden, 'tp', axis=1, tiled=True)  68.6 us
    all_gather x1, waiting for transfers between devices, local(): portion = lax.all_gather(arrived, 'tp', axis=0, tiled=True)  53.9 us
    all_to_all x1, blocking collectives, local(): lax.all_to_all(outgoing, 'sp', split_axis=0, concat_axis=0, tiled=True)  26.7 us
    all_gather x1, waiting for transfers between devices, local(): lax.all_gather(out_weight, 'tp', axis=0, tiled=True)  25.8 us
    all_to_all x1, waiting for transfers between devices, local(): lax.all_to_all(column_out.reshape(tp_count, sp_count, slots_each, column_...  15.9 us
    all_to_all x1, starting transfers between devices, local(): lax.all_to_all(mixer_out, 'tp', split_axis=0, concat_axis=1, tiled=True)  8.07 us
    all_to_all x1, waiting for transfers between devices, local(): lax.all_to_all(combined_cols, 'tp', split_axis=0, concat_axis=1, tiled=True)  7.76 us
    all_to_all x1, waiting for transfers between devices, local(): lax.all_to_all(mixer_out, 'tp', split_axis=0, concat_axis=1, tiled=True)  7.26 us
  transfers between devices with their start and end apart: 7, of which 6 were waited for; matrix products, arithmetic and copies ran while one was open for 3% of the time, Pallas kernels for 0%

commit v1 on v0

v1 whole, which is shorter than its diff:
```python
import functools

import jax
import jax.numpy as jnp
from jax import lax
from jax.experimental import pallas as pl
from jax.experimental.pallas import tpu as pltpu
from jax.sharding import PartitionSpec as P

MESH = pl.DeviceIdType.MESH
F32 = jnp.float32
BF16 = jnp.bfloat16
LIMIT = 7.0
SLOPE = 1.702
EPS = 1e-06
CHUNKS = 4
OPS = (("r", 0), ("r", 1), ("r", 2), ("h", 0), ("r", 3), ("h", 1), ("h", 2), ("h", 3))


def kernel(
    cfg,
    stream, pre, value, post, taps, weight, ids, route_w, ffn_gain, post_gain,
    gate_hbm, up_hbm, down_hbm,
    out,
    halo_src, halo_dst, mixed, w_in, w_diag, s_in, squares, picker, comb_w, slot_cols,
    sent, rows, hidden, result, back, res_keep, res_in, comb_out, comb_in, w_gu, w_down,
    load_sem, halo_sem, small_send, small_recv, mix_recv, disp_recv, ring_recv, ring_pair,
    ring_send, back_recv,
):
    n_sp, n_tp, dim_x, cap = cfg
    dim_z, dim_y = n_sp // dim_x, n_tp // 2
    s, t = lax.axis_index("sp"), lax.axis_index("tp")
    sz, sx = s // dim_x, lax.rem(s, dim_x)
    y, core = t // 2, lax.rem(t, 2)
    n_rows = pre.shape[0]
    own = n_rows // n_tp
    half = n_rows // 2
    block = own * cap * n_tp // own
    slots = block * n_sp
    per_chunk = n_sp // CHUNKS
    chunk = per_chunk * block

    def at_tp(step_y, other_core):
        to_core = 1 - core if other_core else core
        return lax.rem(y + step_y + dim_y, dim_y) * 2 + to_core

    def remote(src, dst, send, recv, tp=None, sp=None):
        target = {"tp": tp} if sp is None else {"sp": sp}
        return pltpu.make_async_remote_copy(
            src_ref=src, dst_ref=dst, send_sem=send, recv_sem=recv,
            device_id=target, device_id_type=MESH,
        )

    def drain(ref, sem):
        pltpu.make_async_copy(ref, ref, sem).wait()

    def z_step(p):
        place = p // dim_x
        return (place + 1) // 2 if place % 2 else (dim_z - place // 2) % dim_z

    loads = [
        pltpu.make_async_copy(gate_hbm.at[0], w_gu.at[:, pl.ds(0, 128)], load_sem.at[0]),
        pltpu.make_async_copy(up_hbm.at[0], w_gu.at[:, pl.ds(128, 128)], load_sem.at[1]),
        pltpu.make_async_copy(down_hbm.at[0], w_down, load_sem.at[2]),
    ]
    for load in loads:
        load.start()

    barrier = pltpu.get_barrier_semaphore()

    def greet_tp(step, carry):
        pl.semaphore_signal(
            barrier, inc=1, device_id={"tp": lax.rem(t + step, n_tp)}, device_id_type=MESH
        )
        return carry

    def greet_sp(step, carry):
        pl.semaphore_signal(
            barrier, inc=1, device_id={"sp": lax.rem(s + step, n_sp)}, device_id_type=MESH
        )
        return carry

    lax.fori_loop(1, n_tp, greet_tp, 0)
    lax.fori_loop(1, n_sp, greet_sp, 0)

    gated = (pre[...].astype(F32) * value[...].astype(F32)).astype(BF16)
    halo_src[:, pl.ds(0, gated.shape[1])] = gated[n_rows - 16 :, :]
    w_diag[...] = jnp.zeros_like(w_diag)

    pl.semaphore_wait(barrier, n_tp + n_sp - 2)

    halo = remote(
        halo_src, halo_dst, halo_sem.at[0], halo_sem.at[1], sp=lax.rem(s + 1, n_sp)
    )
    halo.start()

    tp_steps = [(d, o) for d in (4, 3, 5, 2, 6, 1, 7) for o in (False, True)] + [(0, True)]
    for step_y, other in tp_steps:
        to = at_tp(step_y, other)
        piece = pl.ds(pl.multiple_of(to * 128, 128), 128)
        remote(weight.at[:, piece], w_in.at[t], small_send.at[0], small_recv.at[0], tp=to).start()
    for step_y, other in tp_steps:
        to = at_tp(step_y, other)
        piece = pl.ds(pl.multiple_of(to * 128, 128), 128)
        remote(stream.at[:, piece], s_in.at[t], small_send.at[1], small_recv.at[1], tp=to).start()
    own_cols = pl.ds(pl.multiple_of(t * 128, 128), 128)
    w_in[t] = weight[:, own_cols]
    s_in[t] = stream[:, own_cols]

    wide = gated.astype(F32)
    tap = taps[...].astype(F32)
    row_no = lax.broadcasted_iota(jnp.int32, wide.shape, 0)
    shift_1, shift_2 = pltpu.roll(wide, 1, 0), pltpu.roll(wide, 2, 0)
    halo.wait_recv()
    rim = halo_dst[...].astype(F32)[:, : wide.shape[1]]
    rim = jnp.where(s > 0, rim, 0.0)
    last, before_last = rim[15:16, :], rim[14:15, :]
    shift_1 = jnp.where(row_no == 0, last, shift_1)
    shift_2 = jnp.where(row_no == 0, before_last, jnp.where(row_no == 1, last, shift_2))
    convolved = tap[0:1] * shift_2
    convolved = convolved + tap[1:2] * shift_1
    convolved = convolved + tap[2:3] * wide
    mixer = post[...].astype(F32) * convolved
    mixed[t] = jnp.concatenate([mixer[:half], mixer[half:]], axis=1).astype(BF16)

    steps = (4, 3, 5, 2, 6, 1, 7)
    for step_y in steps:
        remote(
            mixed.at[t], mixed.at[t], small_send.at[2], mix_recv.at[step_y], tp=at_tp(step_y, False)
        ).start()
    partner = at_tp(0, True)
    remote(mixed.at[t], mixed.at[t], small_send.at[2], mix_recv.at[0], tp=partner).start()

    id_cols = ids[...]
    lane = lax.broadcasted_iota(jnp.int32, (n_rows, 128), 1)
    named = jnp.zeros((n_rows, 128), F32)
    for k in range(ids.shape[1]):
        named = named + jnp.where(id_cols[:, k : k + 1] == lane, 1.0, 0.0)
    row_a = lax.broadcasted_iota(jnp.int32, (n_rows, n_rows), 0)
    row_b = lax.broadcasted_iota(jnp.int32, (n_rows, n_rows), 1)
    earlier = jnp.where((row_a > row_b) & (row_a // own == row_b // own), 1.0, 0.0).astype(BF16)
    rank = jnp.dot(earlier, named.astype(BF16), preferred_element_type=F32).astype(jnp.int32)
    dz = lax.rem(sz - lane // dim_x + 32 * dim_z, dim_z)
    dx = lax.rem(sx - lax.rem(lane, dim_x) + 32 * dim_x, dim_x)
    z_place = jnp.where(
        dz * 2 <= dim_z, jnp.maximum(2 * dz - 1, 0), 2 * (dim_z - dz)
    )
    at_lane = lax.broadcasted_iota(jnp.int32, (n_rows, 128), 0)
    slot_of = ((z_place * dim_x + dx) * block + (at_lane // own) * cap + rank).astype(F32)
    columns = jnp.zeros((n_rows, 128), F32)
    for k in range(ids.shape[1]):
        found = jnp.sum(
            jnp.where(id_cols[:, k : k + 1] == lane, slot_of, 0.0), axis=1, keepdims=True
        )
        columns = jnp.where(lane == k, found, columns)
    slot_cols[...] = columns
    slot_rows = jnp.transpose(columns)

    def fill_picker(part, carry):
        first = pl.multiple_of(part * 256, 256)
        number = lax.broadcasted_iota(jnp.int32, (256, n_rows), 0) + part * 256
        number = number.astype(F32)
        hit = number == slot_rows[0:1, :]
        for k in range(1, ids.shape[1]):
            hit = hit | (number == slot_rows[k : k + 1, :])
        picker[pl.ds(first, 256), :] = jnp.where(hit, 1.0, 0.0).astype(BF16)
        return carry

    lax.fori_loop(0, slots // 256, fill_picker, 0)

    drain(w_in.at[pl.ds(0, n_tp - 1)], small_recv.at[0])
    for k in range(n_tp):
        piece = w_in[k]
        w_diag[pl.ds(k * 128, 64), pl.ds(0, 128)] = piece
        w_diag[pl.ds(k * 128 + 64, 64), pl.ds(128, 128)] = piece
    for step_y in steps:
        arrived = mixed.at[at_tp(-step_y, False)]
        drain(arrived, mix_recv.at[step_y])
        remote(arrived, arrived, small_send.at[2], mix_recv.at[0], tp=partner).start()
    drain(s_in.at[pl.ds(0, n_tp - 1)], small_recv.at[1])
    drain(mixed.at[pl.ds(0, dim_y)], mix_recv.at[0])
    stacked = jnp.concatenate([mixed[k] for k in range(n_tp)], axis=1)
    projected = jnp.dot(stacked, w_diag[...], preferred_element_type=F32)
    projected = jnp.concatenate([projected[:, :128], projected[:, 128:]], axis=0)
    residual = (s_in[...].reshape(n_rows, 128).astype(F32) + projected).astype(BF16)
    res_keep[...] = residual
    res = residual.astype(F32)

    sums = jnp.sum(res * res, axis=1, keepdims=True)
    across = jnp.transpose(jnp.broadcast_to(sums, (n_rows, 128)))
    first_row = lax.broadcasted_iota(jnp.int32, (8, half), 0) == 0
    squares[t] = jnp.where(first_row, across[0:8, :half], across[0:8, half:])
    for step_y, other in tp_steps:
        remote(
            squares.at[t], squares.at[t], small_send.at[3], small_recv.at[2],
            tp=at_tp(step_y, other),
        ).start()
    for step_y, other in tp_steps:
        to = at_tp(step_y, other)
        remote(
            res_keep.at[pl.ds(pl.multiple_of(to * own, own), own), :], res_in.at[t],
            small_send.at[4], small_recv.at[3], tp=to,
        ).start()
    res_in[t] = res_keep[pl.ds(pl.multiple_of(t * own, own), own), :]
    drain(squares.at[pl.ds(0, n_tp - 1)], small_recv.at[2])
    total = squares[0]
    for k in range(1, n_tp):
        total = total + squares[k]
    scale = lax.rsqrt(total / (n_tp * 128) + EPS)
    scale = jnp.concatenate(
        [jnp.transpose(jnp.broadcast_to(scale[k : k + 1, :], (half, half))) for k in range(2)], axis=0
    )
    normed = (res * scale * ffn_gain[:, own_cols].astype(F32)).astype(BF16)

    for part in range(CHUNKS):
        span = pl.ds(part * chunk, chunk)
        picked = jnp.dot(picker[span, :], normed, preferred_element_type=F32).astype(BF16)
        sent[span, :] = picked
        if part == 0:
            rows[t, pl.ds(0, block), :] = picked[:block]
        for p in range(max(1, part * per_chunk), (part + 1) * per_chunk):
            to_z = lax.rem(sz - z_step(p) + dim_z, dim_z)
            to_x = lax.rem(sx - p % dim_x + dim_x, dim_x)
            place = pl.ds(p * block, block)
            remote(
                sent.at[place, :], rows.at[t, place, :], small_send.at[5], disp_recv.at[part],
                sp=to_z * dim_x + to_x,
            ).start()

    def fill_weights(part, carry):
        first = pl.multiple_of(part * 256, 256)
        number = lax.broadcasted_iota(jnp.int32, (n_rows, 256), 1) + part * 256
        number = number.astype(F32)
        places = slot_cols[...]
        amounts = route_w[...]
        summed = jnp.zeros((n_rows, 256), F32)
        for k in range(ids.shape[1]):
            summed = summed + jnp.where(
                number == places[:, k : k + 1], amounts[:, k : k + 1], 0.0
            )
        high = summed.astype(BF16)
        comb_w[pl.ds(0, n_rows), pl.ds(first, 256)] = high
        comb_w[pl.ds(n_rows, n_rows), pl.ds(first, 256)] = (summed - high.astype(F32)).astype(BF16)
        return carry

    lax.fori_loop(0, slots // 256, fill_weights, 0)
    for load in loads:
        load.wait()

    lower, upper = chunk // 2, chunk - chunk // 2

    def units(i, part):
        span = pl.ds(i * chunk + part * lower, lower)
        held = jnp.concatenate([rows[k, span, :] for k in range(n_tp)], axis=1)
        both = jnp.dot(held, w_gu[...], preferred_element_type=F32)
        gate = jnp.minimum(both[:, :128], LIMIT)
        up = jnp.clip(both[:, 128:], -LIMIT, LIMIT)
        hidden[t, span, :] = ((up + 1.0) * (gate * jax.nn.sigmoid(SLOPE * gate))).astype(BF16)

    def outputs(i, part):
        span = pl.ds(i * chunk + part * lower, lower)
        held = jnp.concatenate([hidden[k, span, :] for k in range(n_tp)], axis=1)
        result[span, :] = jnp.dot(held, w_down[...], preferred_element_type=F32).astype(BF16)

    def send_back(i):
        for p in range(i * per_chunk, (i + 1) * per_chunk):
            place = pl.ds(p * block, block)
            if p == 0:
                back[place, :] = result[place, :]
                continue
            to_z = lax.rem(sz + z_step(p), dim_z)
            to_x = lax.rem(sx + p % dim_x, dim_x)
            remote(
                result.at[place, :], back.at[place, :], small_send.at[6], back_recv.at[i],
                sp=to_z * dim_x + to_x,
            ).start()

    right, left = at_tp(1, False), at_tp(-1, False)

    def ring_step(j, d):
        kind, i = OPS[j]
        held = rows if kind == "r" else hidden
        full = pl.ds(i * chunk, chunk)
        first = pl.ds(i * chunk, lower)
        second = pl.ds(i * chunk + lower, upper)

        def pass_on(origin, span, to, sem):
            piece = held.at[origin, span, :]
            remote(piece, piece, ring_send.at[j], sem, tp=to).start()

        if d == 0:
            if kind == "r":
                taken = (per_chunk - (1 if i == 0 else 0)) * block
                drain(sent.at[pl.ds(0, taken), :], disp_recv.at[i])
            pass_on(t, full, right, ring_recv.at[j, 0, 0])
            pass_on(t, full, left, ring_recv.at[j, 1, 0])
            pass_on(t, full, partner, ring_pair.at[j])
            return
        for way, sign, ahead, end in ((0, -1, right, first), (1, 1, left, second)):
            origin = at_tp(sign * d, False)
            span = full if d < 4 else end
            drain(held.at[origin, span, :], ring_recv.at[j, way, d - 1])
            if d < 4:
                pass_on(origin, full if d < 3 else end, ahead, ring_recv.at[j, way, d])
            pass_on(origin, span, partner, ring_pair.at[j])
        if d == 4:
            drain(held.at[pl.ds(0, dim_y), full, :], ring_pair.at[j])

    work = {
        4: [(units, 0, 0)], 5: [(units, 0, 1)],
        7: [(units, 1, 0)], 8: [(units, 1, 1)],
        9: [(units, 2, 0)],
        10: [(outputs, 0, 0), (outputs, 0, 1)],
        11: [(units, 2, 1)],
        12: [(units, 3, 0)], 13: [(units, 3, 1)],
        14: [(outputs, 1, 0), (outputs, 1, 1)],
        16: [(outputs, 2, 0), (outputs, 2, 1)],
        18: [(outputs, 3, 0), (outputs, 3, 1)],
    }
    for slot in range(2 * len(OPS) + 3):
        for j in range(len(OPS)):
            d = slot - 2 * j
            if 0 <= d <= 4:
                ring_step(j, d)
        for task, i, part in work.get(slot, ()):
            task(i, part)
            if task is outputs and part == 1:
                send_back(i)

    summed = jnp.zeros((2 * n_rows, 128), F32)
    for i in range(CHUNKS):
        taken = (per_chunk - (1 if i == 0 else 0)) * block
        drain(back.at[pl.ds(0, taken), :], back_recv.at[i])
        span = pl.ds(i * chunk, chunk)
        summed = summed + jnp.dot(comb_w[:, span], back[span, :], preferred_element_type=F32)
    comb_out[...] = (summed[:n_rows] + summed[n_rows:]).astype(BF16)
    for step_y, other in tp_steps:
        to = at_tp(step_y, other)
        remote(
            comb_out.at[pl.ds(pl.multiple_of(to * own, own), own), :], comb_in.at[t],
            small_send.at[7], small_recv.at[4], tp=to,
        ).start()
    comb_in[t] = comb_out[pl.ds(pl.multiple_of(t * own, own), own), :]

    halo.wait_send()
    drain(w_in.at[pl.ds(0, n_tp - 1)], small_send.at[0])
    drain(s_in.at[pl.ds(0, n_tp - 1)], small_send.at[1])
    drain(mixed.at[pl.ds(0, 2 * dim_y - 1)], small_send.at[2])
    drain(squares.at[pl.ds(0, n_tp - 1)], small_send.at[3])
    drain(res_in.at[pl.ds(0, n_tp - 1)], small_send.at[4])
    drain(sent.at[pl.ds(0, slots - block), :], small_send.at[5])
    drain(result.at[pl.ds(0, slots - block), :], small_send.at[6])
    for j in range(len(OPS)):
        drain(rows.at[pl.ds(0, 15), pl.ds(0, chunk), :], ring_send.at[j])

    drain(res_in.at[pl.ds(0, n_tp - 1)], small_recv.at[3])
    drain(comb_in.at[pl.ds(0, n_tp - 1)], small_recv.at[4])
    drain(comb_in.at[pl.ds(0, n_tp - 1)], small_send.at[7])
    combined = jnp.concatenate([comb_in[k] for k in range(n_tp)], axis=1).astype(F32)
    kept = jnp.concatenate([res_in[k] for k in range(n_tp)], axis=1).astype(F32)
    mean = jnp.mean(combined * combined, axis=1, keepdims=True)
    out[...] = (kept + combined * lax.rsqrt(mean + EPS) * post_gain[...].astype(F32)).astype(BF16)


def local(
    stream_in, pre_gate, value_in, post_gate, conv_taps, out_weight, route_ids, route_weight,
    ffn_gain, post_gain, gate_proj, up_proj, down_proj,
):
    n_sp, n_tp = lax.axis_size("sp"), lax.axis_size("tp")
    own, features = stream_in.shape
    n_rows = pre_gate.shape[0]
    cap = 2 * own * route_ids.shape[1] // n_sp
    slots = n_sp * n_tp * cap
    vmem = pl.BlockSpec(memory_space=pltpu.VMEM)
    hbm = pl.BlockSpec(memory_space=pl.ANY)
    dma = pltpu.SemaphoreType.DMA
    chunks = CHUNKS
    return pl.pallas_call(
        functools.partial(kernel, (n_sp, n_tp, 4, cap)),
        out_shape=jax.ShapeDtypeStruct(stream_in.shape, BF16),
        in_specs=[vmem] * 10 + [hbm] * 3,
        out_specs=vmem,
        scratch_shapes=[
            pltpu.VMEM((16, 128), BF16),
            pltpu.VMEM((16, 128), BF16),
            pltpu.VMEM((n_tp, n_rows // 2, 128), BF16),
            pltpu.VMEM((n_tp, 64, 128), BF16),
            pltpu.VMEM((n_tp * 128, 256), BF16),
            pltpu.VMEM((n_tp, own, 128), BF16),
            pltpu.VMEM((n_tp, 8, n_rows // 2), F32),
            pltpu.VMEM((slots, n_rows), BF16),
            pltpu.VMEM((2 * n_rows, slots), BF16),
            pltpu.VMEM((n_rows, 128), F32),
            pltpu.VMEM((slots, 128), BF16),
            pltpu.VMEM((n_tp, slots, 128), BF16),
            pltpu.VMEM((n_tp, slots, 128), BF16),
            pltpu.VMEM((slots, 128), BF16),
            pltpu.VMEM((slots, 128), BF16),
            pltpu.VMEM((n_rows, 128), BF16),
            pltpu.VMEM((n_tp, own, 128), BF16),
            pltpu.VMEM((n_rows, 128), BF16),
            pltpu.VMEM((n_tp, own, 128), BF16),
            pltpu.VMEM((features, 256), BF16),
            pltpu.VMEM((features, 128), BF16),
            dma((3,)), dma((2,)), dma((8,)), dma((5,)), dma((8,)), dma((chunks,)),
            dma((len(OPS), 2, 4)), dma((len(OPS),)), dma((len(OPS),)), dma((chunks,)),
        ],
        compiler_params=pltpu.CompilerParams(
            collective_id=0, has_side_effects=True, vmem_limit_bytes=56 * 1024 * 1024
        ),
        cost_estimate=pl.CostEstimate(flops=4 * 10**9, bytes_accessed=3 * 10**6, transcendentals=0),
    )(
        stream_in, pre_gate, value_in, post_gate, conv_taps, out_weight, route_ids, route_weight,
        ffn_gain.reshape(1, features), post_gain.reshape(1, features),
        gate_proj, up_proj, down_proj,
    )


def solution(mesh):
    placed = (
        P(("sp", "tp"), None),
        P("sp", "tp"),
        P("sp", "tp"),
        P("sp", "tp"),
        P(None, "tp"),
        P("tp", None),
        P("sp", None),
        P("sp", None),
        P(),
        P(),
        P("sp", None, "tp"),
        P("sp", None, "tp"),
        P("sp", None, "tp"),
    )
    return jax.shard_map(
        local, mesh=mesh, in_specs=placed, out_specs=P(("sp", "tp"), None), check_vma=False
    )
```

time: 281 us -> 172 us (0.61)
  waiting for transfers between devices: 180 us -> 0 us
  Pallas kernels: 0 us -> 164 us
  blocking collectives: 26.7 us -> 0 us
  starting transfers between devices: 25.4 us -> 0 us
  matrix products: 18.2 us -> 0 us
  between operations: 13.4 us -> 0.02 us
  other arithmetic: 7.76 us -> 0 us
    pallas_call x0 -> x1, Pallas kernels: none -> 164 us  [local(): pl.pallas_call(functools.partial(kernel, (n_sp, n_tp, 4, cap)), out_shape...]
    all_gather x3 -> x0, waiting for transfers between devices: 148 us -> none  [the longest x1 68.6 us: local(): lax.all_gather(hidden, 'tp', axis=1, tiled=True)]
    all_to_all x3 -> x0, waiting for transfers between devices: 30.9 us -> none  [the longest x1 15.9 us: local(): lax.all_to_all(column_out.reshape(tp_count, sp_count, slots_each, column_...]
    all_to_all x1 -> x0, blocking collectives: 26.7 us -> none  [local(): lax.all_to_all(outgoing, 'sp', split_axis=0, concat_axis=0, tiled=True)]
    all_to_all x3 -> x0, starting transfers between devices: 21.4 us -> none  [the longest x1 8.07 us: local(): lax.all_to_all(mixer_out, 'tp', split_axis=0, concat_axis=1, tiled=True)]
    dot_general x5 -> x0, matrix products: 18.2 us -> none  [the longest x1 5.91 us: local(): jnp.dot(portion, gate_proj[0], preferred_element_type=jnp.float32)]
    unnamed x18 -> x16, local copies, waits for them, and re-layouts: 1.82 us -> 6.06 us
    ppermute x1 -> x0, starting transfers between devices: 3.92 us -> none  [passed_along(): return lax.ppermute(array, axis, pairs)]
  transfers between devices with their start and end apart: 7 -> 0, of which waited for: 6 -> 0; matrix products, arithmetic and copies ran while one was open for 3% -> 0% of each run, Pallas kernels for 0% -> 0%
where the time goes in v1:
time: 172 us
  Pallas kernels  164 us (95%)
  local copies, waits for them, and re-layouts  7.96 us (5%)
    pallas_call x1, Pallas kernels, local(): pl.pallas_call(functools.partial(kernel, (n_sp, n_tp, 4, cap)), out_shape...  164 us
    unnamed x16, local copies, waits for them, and re-layouts  6.06 us

profile of v1, /device:TPU:1, one launch (start us, length us, event | category | flops | bytes accessed | tf_op | source)
XLA Modules:
  0.0 171.5 jit_solution(6069310477840076929)
XLA Ops:
  0.0 0.0 copy-start.2
  0.0 1.3 reshape.6.ffn_gain
  1.3 0.0 copy-done.2
  1.3 0.6 reshape.7.post_gain
  1.9 0.0 copy-start
  1.9 1.5 copy.14.pre
  3.4 0.0 copy-done
  3.4 0.0 copy-start.1
  3.4 0.7 copy.15.value
  4.1 0.0 copy-done.1
  4.2 0.0 copy-start.3
  4.2 0.7 copy.16.post
  4.9 0.0 copy-done.3
  4.9 0.0 copy-start.4
  4.9 0.8 copy.17.ids
  5.7 0.0 copy-done.4
  5.7 0.8 copy.18.route_w
  6.5 163.6 %shard_map.127 = bf16[16,2048]{1,0:T(8,128)(2,1)} custom-call(bf16[16,2048]{1,0:T(8,128)(2,1)} %stream.1, bf16[256,64]{1,0:T(8,128)(2,1)} %copy.14.pre, bf16[256,64]{1,0:T(8,128)(2,1)} %copy.15.value, bf16[256,64]{1,0:T(8,128)(2,1)} %copy.16.post, bf16[3,64]{1,0:T(4,128)(2,1)} %taps.1, bf16[64,2048]{1,0:T(8,128)(2,1)} %weight.1, s32[256,4]{1,0:T(8,128)} %copy.17.ids, ...), custom_call_target="tpu_custom_call" | custom-call | flops 4000000000 | bytes 3000000 | tf_op jit(solution)/shard_map/pallas_call | solution.py:378
  170.1 1.5 copy.20
Async XLA Ops:
  0.0 1.3 copy-start.2
  1.9 1.5 copy-start
  3.4 0.8 copy-start.1
  4.2 0.7 copy-start.3
  4.9 0.8 copy-start.4

commit v2 on v1

--- a/solution.py
+++ b/solution.py
@@ -14,7 +14,8 @@
 SLOPE = 1.702
 EPS = 1e-06
 CHUNKS = 4
-OPS = (("r", 0), ("r", 1), ("r", 2), ("h", 0), ("r", 3), ("h", 1), ("h", 2), ("h", 3))
+OPS = (("r", 0), ("r", 1), ("r", 2), ("r", 3), ("h", 0), ("h", 1), ("h", 2), ("h", 3))
+STARTS = (0, 1, 2, 3, 5, 6, 7, 8)
 
 
 def kernel(
@@ -22,7 +23,7 @@
     stream, pre, value, post, taps, weight, ids, route_w, ffn_gain, post_gain,
     gate_hbm, up_hbm, down_hbm,
     out,
-    halo_src, halo_dst, mixed, w_in, w_diag, s_in, squares, picker, comb_w, slot_cols,
+    halo_src, halo_dst, mixed, w_in, w_diag, s_in, squares, picker, comb_w, aux, slot_cols,
     sent, rows, hidden, result, back, res_keep, res_in, comb_out, comb_in, w_gu, w_down,
     load_sem, halo_sem, small_send, small_recv, mix_recv, disp_recv, ring_recv, ring_pair,
     ring_send, back_recv,
@@ -32,7 +33,9 @@
     s, t = lax.axis_index("sp"), lax.axis_index("tp")
     sz, sx = s // dim_x, lax.rem(s, dim_x)
     y, core = t // 2, lax.rem(t, 2)
-    n_rows = pre.shape[0]
+    n_rows = pre.shape[1]
+    channels = pre.shape[0]
+    top = ids.shape[0]
     own = n_rows // n_tp
     half = n_rows // 2
     block = own * cap * n_tp // own
@@ -83,9 +86,9 @@
     lax.fori_loop(1, n_tp, greet_tp, 0)
     lax.fori_loop(1, n_sp, greet_sp, 0)
 
-    gated = (pre[...].astype(F32) * value[...].astype(F32)).astype(BF16)
-    halo_src[:, pl.ds(0, gated.shape[1])] = gated[n_rows - 16 :, :]
-    w_diag[...] = jnp.zeros_like(w_diag)
+    gated = (pre[...].astype(F32) * value[...].astype(F32)).astype(BF16).astype(F32)
+    gates = jnp.transpose(jnp.concatenate([gated, post[...].astype(F32)], axis=0))
+    halo_src[...] = gates[n_rows - 16 :, :].astype(BF16)
 
     pl.semaphore_wait(barrier, n_tp + n_sp - 2)
 
@@ -107,12 +110,44 @@
     w_in[t] = weight[:, own_cols]
     s_in[t] = stream[:, own_cols]
 
-    wide = gated.astype(F32)
+    aux[...] = jnp.zeros_like(aux)
+    aux[0:top, :] = ids[...].astype(F32)
+    aux[top : 2 * top, :] = route_w[...]
+    by_row = jnp.transpose(aux[...])
+    id_cols = [by_row[:, k : k + 1] for k in range(top)]
+    amounts = [by_row[:, top + k : top + k + 1] for k in range(top)]
+    lane = lax.broadcasted_iota(jnp.int32, (n_rows, 128), 1)
+    lane_f = lane.astype(F32)
+    named = jnp.zeros((n_rows, 128), F32)
+    for k in range(top):
+        named = named + jnp.where(id_cols[k] == lane_f, 1.0, 0.0)
+    row_a = lax.broadcasted_iota(jnp.int32, (n_rows, n_rows), 0)
+    row_b = lax.broadcasted_iota(jnp.int32, (n_rows, n_rows), 1)
+    earlier = jnp.where((row_a > row_b) & (row_a // own == row_b // own), 1.0, 0.0).astype(BF16)
+    rank = jnp.dot(earlier, named.astype(BF16), preferred_element_type=F32)
+    dz = lax.rem(sz - lane // dim_x + 32 * dim_z, dim_z)
+    dx = lax.rem(sx - lax.rem(lane, dim_x) + 32 * dim_x, dim_x)
+    z_place = jnp.where(dz * 2 <= dim_z, jnp.maximum(2 * dz - 1, 0), 2 * (dim_z - dz))
+    at_row = lax.broadcasted_iota(jnp.int32, (n_rows, 128), 0)
+    slot_of = ((z_place * dim_x + dx) * block + (at_row // own) * cap).astype(F32) + rank
+    places = [
+        jnp.sum(jnp.where(id_cols[k] == lane_f, slot_of, 0.0), axis=1, keepdims=True)
+        for k in range(top)
+    ]
+    columns = jnp.zeros((n_rows, 128), F32)
+    for k in range(top):
+        columns = jnp.where(lane == k, places[k], columns)
+        columns = jnp.where(lane == top + k, amounts[k], columns)
+    slot_cols[...] = columns
+    slot_rows = jnp.transpose(columns)
+    w_diag[...] = jnp.zeros_like(w_diag)
+
+    wide, second = gates[:, :channels], gates[:, channels:]
     tap = taps[...].astype(F32)
     row_no = lax.broadcasted_iota(jnp.int32, wide.shape, 0)
     shift_1, shift_2 = pltpu.roll(wide, 1, 0), pltpu.roll(wide, 2, 0)
     halo.wait_recv()
-    rim = halo_dst[...].astype(F32)[:, : wide.shape[1]]
+    rim = halo_dst[...].astype(F32)[:, :channels]
     rim = jnp.where(s > 0, rim, 0.0)
     last, before_last = rim[15:16, :], rim[14:15, :]
     shift_1 = jnp.where(row_no == 0, last, shift_1)
@@ -120,7 +155,7 @@
     convolved = tap[0:1] * shift_2
     convolved = convolved + tap[1:2] * shift_1
     convolved = convolved + tap[2:3] * wide
-    mixer = post[...].astype(F32) * convolved
+    mixer = second * convolved
     mixed[t] = jnp.concatenate([mixer[:half], mixer[half:]], axis=1).astype(BF16)
 
     steps = (4, 3, 5, 2, 6, 1, 7)
@@ -131,37 +166,12 @@
     partner = at_tp(0, True)
     remote(mixed.at[t], mixed.at[t], small_send.at[2], mix_recv.at[0], tp=partner).start()
 
-    id_cols = ids[...]
-    lane = lax.broadcasted_iota(jnp.int32, (n_rows, 128), 1)
-    named = jnp.zeros((n_rows, 128), F32)
-    for k in range(ids.shape[1]):
-        named = named + jnp.where(id_cols[:, k : k + 1] == lane, 1.0, 0.0)
-    row_a = lax.broadcasted_iota(jnp.int32, (n_rows, n_rows), 0)
-    row_b = lax.broadcasted_iota(jnp.int32, (n_rows, n_rows), 1)
-    earlier = jnp.where((row_a > row_b) & (row_a // own == row_b // own), 1.0, 0.0).astype(BF16)
-    rank = jnp.dot(earlier, named.astype(BF16), preferred_element_type=F32).astype(jnp.int32)
-    dz = lax.rem(sz - lane // dim_x + 32 * dim_z, dim_z)
-    dx = lax.rem(sx - lax.rem(lane, dim_x) + 32 * dim_x, dim_x)
-    z_place = jnp.where(
-        dz * 2 <= dim_z, jnp.maximum(2 * dz - 1, 0), 2 * (dim_z - dz)
-    )
-    at_lane = lax.broadcasted_iota(jnp.int32, (n_rows, 128), 0)
-    slot_of = ((z_place * dim_x + dx) * block + (at_lane // own) * cap + rank).astype(F32)
-    columns = jnp.zeros((n_rows, 128), F32)
-    for k in range(ids.shape[1]):
-        found = jnp.sum(
-            jnp.where(id_cols[:, k : k + 1] == lane, slot_of, 0.0), axis=1, keepdims=True
-        )
-        columns = jnp.where(lane == k, found, columns)
-    slot_cols[...] = columns
-    slot_rows = jnp.transpose(columns)
-
     def fill_picker(part, carry):
         first = pl.multiple_of(part * 256, 256)
         number = lax.broadcasted_iota(jnp.int32, (256, n_rows), 0) + part * 256
         number = number.astype(F32)
         hit = number == slot_rows[0:1, :]
-        for k in range(1, ids.shape[1]):
+        for k in range(1, top):
             hit = hit | (number == slot_rows[k : k + 1, :])
         picker[pl.ds(first, 256), :] = jnp.where(hit, 1.0, 0.0).astype(BF16)
         return carry
@@ -195,13 +205,6 @@
             squares.at[t], squares.at[t], small_send.at[3], small_recv.at[2],
             tp=at_tp(step_y, other),
         ).start()
-    for step_y, other in tp_steps:
-        to = at_tp(step_y, other)
-        remote(
-            res_keep.at[pl.ds(pl.multiple_of(to * own, own), own), :], res_in.at[t],
-            small_send.at[4], small_recv.at[3], tp=to,
-        ).start()
-    res_in[t] = res_keep[pl.ds(pl.multiple_of(t * own, own), own), :]
     drain(squares.at[pl.ds(0, n_tp - 1)], small_recv.at[2])
     total = squares[0]
     for k in range(1, n_tp):
@@ -210,7 +213,10 @@
     scale = jnp.concatenate(
         [jnp.transpose(jnp.broadcast_to(scale[k : k + 1, :], (half, half))) for k in range(2)], axis=0
     )
-    normed = (res * scale * ffn_gain[:, own_cols].astype(F32)).astype(BF16)
+    gains = ffn_gain[...].astype(F32).reshape(n_tp, 128)
+    gain_no = lax.broadcasted_iota(jnp.int32, (n_tp, 128), 0)
+    gain = jnp.sum(jnp.where(gain_no == t, gains, 0.0), axis=0, keepdims=True)
+    normed = (res * scale * gain).astype(BF16)
 
     for part in range(CHUNKS):
         span = pl.ds(part * chunk, chunk)
@@ -227,23 +233,32 @@
                 sp=to_z * dim_x + to_x,
             ).start()
 
+    for step_y, other in tp_steps:
+        to = at_tp(step_y, other)
+        remote(
+            res_keep.at[pl.ds(pl.multiple_of(to * own, own), own), :], res_in.at[t],
+            small_send.at[4], small_recv.at[3], tp=to,
+        ).start()
+    res_in[t] = res_keep[pl.ds(pl.multiple_of(t * own, own), own), :]
+
     def fill_weights(part, carry):
         first = pl.multiple_of(part * 256, 256)
         number = lax.broadcasted_iota(jnp.int32, (n_rows, 256), 1) + part * 256
         number = number.astype(F32)
-        places = slot_cols[...]
-        amounts = route_w[...]
+        columns = slot_cols[...]
         summed = jnp.zeros((n_rows, 256), F32)
-        for k in range(ids.shape[1]):
+        for k in range(top):
             summed = summed + jnp.where(
-                number == places[:, k : k + 1], amounts[:, k : k + 1], 0.0
+                number == columns[:, k : k + 1], columns[:, top + k : top + k + 1], 0.0
             )
         high = summed.astype(BF16)
         comb_w[pl.ds(0, n_rows), pl.ds(first, 256)] = high
         comb_w[pl.ds(n_rows, n_rows), pl.ds(first, 256)] = (summed - high.astype(F32)).astype(BF16)
         return carry
 
-    lax.fori_loop(0, slots // 256, fill_weights, 0)
+    def weights(i, part):
+        lax.fori_loop(0, slots // 256, fill_weights, 0)
+
     for load in loads:
         load.wait()
 
@@ -306,20 +321,13 @@
         if d == 4:
             drain(held.at[pl.ds(0, dim_y), full, :], ring_pair.at[j])
 
-    work = {
-        4: [(units, 0, 0)], 5: [(units, 0, 1)],
-        7: [(units, 1, 0)], 8: [(units, 1, 1)],
-        9: [(units, 2, 0)],
-        10: [(outputs, 0, 0), (outputs, 0, 1)],
-        11: [(units, 2, 1)],
-        12: [(units, 3, 0)], 13: [(units, 3, 1)],
-        14: [(outputs, 1, 0), (outputs, 1, 1)],
-        16: [(outputs, 2, 0), (outputs, 2, 1)],
-        18: [(outputs, 3, 0), (outputs, 3, 1)],
-    }
-    for slot in range(2 * len(OPS) + 3):
+    work = {2: [(weights, 0, 0)]}
+    for i in range(CHUNKS):
+        work.setdefault(4 + i, []).extend([(units, i, 0), (units, i, 1)])
+        work.setdefault(9 + i, []).extend([(outputs, i, 0), (outputs, i, 1)])
+    for slot in range(STARTS[-1] + 5):
         for j in range(len(OPS)):
-            d = slot - 2 * j
+            d = slot - STARTS[j]
             if 0 <= d <= 4:
                 ring_step(j, d)
         for task, i, part in work.get(slot, ()):
@@ -359,7 +367,7 @@
     combined = jnp.concatenate([comb_in[k] for k in range(n_tp)], axis=1).astype(F32)
     kept = jnp.concatenate([res_in[k] for k in range(n_tp)], axis=1).astype(F32)
     mean = jnp.mean(combined * combined, axis=1, keepdims=True)
-    out[...] = (kept + combined * lax.rsqrt(mean + EPS) * post_gain[...].astype(F32)).astype(BF16)
+    out[...] = (kept + combined * lax.rsqrt(mean + EPS) * post_gain[...].astype(F32)[None, :]).astype(BF16)
 
 
 def local(
@@ -390,6 +398,7 @@
             pltpu.VMEM((n_tp, 8, n_rows // 2), F32),
             pltpu.VMEM((slots, n_rows), BF16),
             pltpu.VMEM((2 * n_rows, slots), BF16),
+            pltpu.VMEM((128, n_rows), F32),
             pltpu.VMEM((n_rows, 128), F32),
             pltpu.VMEM((slots, 128), BF16),
             pltpu.VMEM((n_tp, slots, 128), BF16),
@@ -410,8 +419,9 @@
         ),
         cost_estimate=pl.CostEstimate(flops=4 * 10**9, bytes_accessed=3 * 10**6, transcendentals=0),
     )(
-        stream_in, pre_gate, value_in, post_gate, conv_taps, out_weight, route_ids, route_weight,
-        ffn_gain.reshape(1, features), post_gain.reshape(1, features),
+        stream_in, pre_gate.T, value_in.T, post_gate.T, conv_taps, out_weight,
+        route_ids.T, route_weight.T,
+        ffn_gain, post_gain,
         gate_proj, up_proj, down_proj,
     )
 

time: 172 us -> 148 us (0.86)
  Pallas kernels: 164 us -> 146 us
  local copies, waits for them, and re-layouts: 7.96 us -> 1.47 us
    pallas_call x1, Pallas kernels: 164 us -> 146 us  [local(): pl.pallas_call(functools.partial(kernel, (n_sp, n_tp, 4, cap)), out_shape...]
    unnamed x16 -> x1, local copies, waits for them, and re-layouts: 6.06 us -> 1.47 us
    reshape x2 -> x0, local copies, waits for them, and re-layouts: 1.9 us -> none  [the longest x1 1.3 us: local(): ffn_gain.reshape(1, features)]
where the time goes in v2:
time: 148 us
  Pallas kernels  146 us (99%)
    pallas_call x1, Pallas kernels, local(): pl.pallas_call(functools.partial(kernel, (n_sp, n_tp, 4, cap)), out_shape...  146 us

profile of v2, /device:TPU:1, one launch (start us, length us, event | category | flops | bytes accessed | tf_op | source)
XLA Modules:
  0.0 147.9 jit_solution(13215706636832915569)
XLA Ops:
  0.0 146.4 %shard_map.127 = bf16[16,2048]{1,0:T(8,128)(2,1)} custom-call(bf16[16,2048]{1,0:T(8,128)(2,1)} %stream.1, bf16[64,256]{1,0:T(8,128)(2,1)} %bitcast.5, bf16[64,256]{1,0:T(8,128)(2,1)} %bitcast.6, bf16[64,256]{1,0:T(8,128)(2,1)} %bitcast.7, bf16[3,64]{1,0:T(4,128)(2,1)} %taps.1, bf16[64,2048]{1,0:T(8,128)(2,1)} %weight.1, s32[4,256]{1,0:T(4,128)} %bitcast.8, ...), custom_call_target="tpu_custom_call" | custom-call | flops 4000000000 | bytes 3000000 | tf_op jit(solution)/shard_map/pallas_call | solution.py:386
  146.4 1.5 copy.15

commit v3 on v2

--- a/solution.py
+++ b/solution.py
@@ -13,9 +13,13 @@
 LIMIT = 7.0
 SLOPE = 1.702
 EPS = 1e-06
-CHUNKS = 4
-OPS = (("r", 0), ("r", 1), ("r", 2), ("r", 3), ("h", 0), ("h", 1), ("h", 2), ("h", 3))
-STARTS = (0, 1, 2, 3, 5, 6, 7, 8)
+OFFSETS = (0, 1, -1, 2, -2, 3, -3, 4)
+AT = {offset: place for place, offset in enumerate(OFFSETS)}
+NEAR, FAR = (0, 1, 2, 3, 4), (5, 6, 7)
+EARLY, LATE = (0, 1, 2), (3, 4)
+FIRST_SLICES = 3
+OPS = (('g', 0, 0), ('r', 5, 2), ('r', 6, 3), ('r', 7, 4), ('h', 5, 7), ('h', 6, 8), ('h', 7, 9), ('h', 0, 10), ('h', 1, 11), ('h', 2, 12), ('h', 3, 13), ('h', 4, 14))
+WORK = {1: [('pick', 0)], 3: [('weights', 0)], 4: [('pick', 1)], 6: [('units', 5)], 7: [('units', 6)], 8: [('units', 7), ('across', 0)], 9: [('units', 0), ('across', 1)], 10: [('units', 1), ('across', 2)], 11: [('units', 2), ('across', 3)], 12: [('units', 3), ('across', 4)], 13: [('units', 4)]}
 
 
 def kernel(
@@ -24,9 +28,9 @@
     gate_hbm, up_hbm, down_hbm,
     out,
     halo_src, halo_dst, mixed, w_in, w_diag, s_in, squares, picker, comb_w, aux, slot_cols,
-    sent, rows, hidden, result, back, res_keep, res_in, comb_out, comb_in, w_gu, w_down,
-    load_sem, halo_sem, small_send, small_recv, mix_recv, disp_recv, ring_recv, ring_pair,
-    ring_send, back_recv,
+    norms, far_out, near_out, rows, hidden, result, back, res_keep, res_in, comb_out, comb_in, w_gu, w_down,
+    load_sem, halo_sem, small_send, small_recv, mix_recv, far_recv, near_recv, near_pair,
+    ring_recv, ring_pair, ring_send, back_recv,
 ):
     n_sp, n_tp, dim_x, cap = cfg
     dim_z, dim_y = n_sp // dim_x, n_tp // 2
@@ -40,8 +44,7 @@
     half = n_rows // 2
     block = own * cap * n_tp // own
     slots = block * n_sp
-    per_chunk = n_sp // CHUNKS
-    chunk = per_chunk * block
+    zone = dim_x * block
 
     def at_tp(step_y, other_core):
         to_core = 1 - core if other_core else core
@@ -61,13 +64,19 @@
         place = p // dim_x
         return (place + 1) // 2 if place % 2 else (dim_z - place // 2) % dim_z
 
-    loads = [
-        pltpu.make_async_copy(gate_hbm.at[0], w_gu.at[:, pl.ds(0, 128)], load_sem.at[0]),
-        pltpu.make_async_copy(up_hbm.at[0], w_gu.at[:, pl.ds(128, 128)], load_sem.at[1]),
-        pltpu.make_async_copy(down_hbm.at[0], w_down, load_sem.at[2]),
-    ]
-    for load in loads:
-        load.start()
+    for core_no in range(2):
+        for place, offset in enumerate(OFFSETS):
+            origin = pl.ds(pl.multiple_of(at_tp(offset, core_no == 1) * 128, 128), 128)
+            here = pl.ds((core_no * dim_y + place) * 128, 128)
+            pltpu.make_async_copy(
+                gate_hbm.at[0, origin, :], w_gu.at[here, pl.ds(0, 128)], load_sem.at[0]
+            ).start()
+            pltpu.make_async_copy(
+                up_hbm.at[0, origin, :], w_gu.at[here, pl.ds(128, 128)], load_sem.at[1]
+            ).start()
+            pltpu.make_async_copy(
+                down_hbm.at[0, origin, :], w_down.at[here, :], load_sem.at[2]
+            ).start()
 
     barrier = pltpu.get_barrier_semaphore()
 
@@ -97,17 +106,21 @@
     )
     halo.start()
 
+    share = weight.shape[0] // dim_x
+    quarter = pl.ds(pl.multiple_of(sx * share, share), share)
     tp_steps = [(d, o) for d in (4, 3, 5, 2, 6, 1, 7) for o in (False, True)] + [(0, True)]
     for step_y, other in tp_steps:
         to = at_tp(step_y, other)
         piece = pl.ds(pl.multiple_of(to * 128, 128), 128)
-        remote(weight.at[:, piece], w_in.at[t], small_send.at[0], small_recv.at[0], tp=to).start()
+        remote(
+            weight.at[quarter, piece], w_in.at[sx, t], small_send.at[0], small_recv.at[0], tp=to
+        ).start()
     for step_y, other in tp_steps:
         to = at_tp(step_y, other)
         piece = pl.ds(pl.multiple_of(to * 128, 128), 128)
         remote(stream.at[:, piece], s_in.at[t], small_send.at[1], small_recv.at[1], tp=to).start()
     own_cols = pl.ds(pl.multiple_of(t * 128, 128), 128)
-    w_in[t] = weight[:, own_cols]
+    w_in[sx, t] = weight[quarter, own_cols]
     s_in[t] = stream[:, own_cols]
 
     aux[...] = jnp.zeros_like(aux)
@@ -165,6 +178,12 @@
         ).start()
     partner = at_tp(0, True)
     remote(mixed.at[t], mixed.at[t], small_send.at[2], mix_recv.at[0], tp=partner).start()
+    drain(w_in.at[sx, pl.ds(0, n_tp - 1)], small_recv.at[0])
+    for step_x in (2, 1, 3):
+        remote(
+            w_in.at[sx], w_in.at[sx], small_send.at[10], small_recv.at[5],
+            sp=sz * dim_x + lax.rem(sx + step_x, dim_x),
+        ).start()
 
     def fill_picker(part, carry):
         first = pl.multiple_of(part * 256, 256)
@@ -178,9 +197,9 @@
 
     lax.fori_loop(0, slots // 256, fill_picker, 0)
 
-    drain(w_in.at[pl.ds(0, n_tp - 1)], small_recv.at[0])
+    drain(w_in.at[pl.ds(0, dim_x - 1)], small_recv.at[5])
     for k in range(n_tp):
-        piece = w_in[k]
+        piece = jnp.concatenate([w_in[x, k] for x in range(dim_x)], axis=0)
         w_diag[pl.ds(k * 128, 64), pl.ds(0, 128)] = piece
         w_diag[pl.ds(k * 128 + 64, 64), pl.ds(128, 128)] = piece
     for step_y in steps:
@@ -218,20 +237,111 @@
     gain = jnp.sum(jnp.where(gain_no == t, gains, 0.0), axis=0, keepdims=True)
     normed = (res * scale * gain).astype(BF16)
 
-    for part in range(CHUNKS):
-        span = pl.ds(part * chunk, chunk)
-        picked = jnp.dot(picker[span, :], normed, preferred_element_type=F32).astype(BF16)
-        sent[span, :] = picked
-        if part == 0:
-            rows[t, pl.ds(0, block), :] = picked[:block]
-        for p in range(max(1, part * per_chunk), (part + 1) * per_chunk):
-            to_z = lax.rem(sz - z_step(p) + dim_z, dim_z)
-            to_x = lax.rem(sx - p % dim_x + dim_x, dim_x)
+    norms[0] = normed
+
+    right, left = at_tp(1, False), at_tp(-1, False)
+    lower, upper = zone // 2, zone - zone // 2
+
+    def ring_step(j, d):
+        kind, z, _ = OPS[j]
+        base = 0 if kind == "g" else z * zone
+
+        def part(place, span, core_no=0):
+            first, size = span
+            span = pl.ds(base + first, size)
+            if kind == "g":
+                return norms.at[place, span, :]
+            return (rows if kind == "r" else hidden).at[core_no, place, span, :]
+
+        def pass_on(origin, shifted, span, to, sem):
+            remote(part(origin, span), part(shifted, span), ring_send.at[j], sem, tp=to).start()
+
+        def cross(place, span):
+            if kind != "g":
+                remote(
+                    part(place, span), part(place, span, 1), ring_send.at[j], ring_pair.at[j],
+                    tp=partner,
+                ).start()
+
+        full, first, second = (0, zone), (0, lower), (lower, upper)
+        if d == 0:
+            if kind == "r":
+                drain(part(0, full), far_recv.at[z - FAR[0]])
+            pass_on(AT[0], AT[-1], full, right, ring_recv.at[j, 0, 0])
+            pass_on(AT[0], AT[1], full, left, ring_recv.at[j, 1, 0])
+            cross(AT[0], full)
+            return
+        for way, sign, ahead, end in ((0, -1, right, first), (1, 1, left, second)):
+            origin = AT[sign * d] if d < 4 else AT[4]
+            span = full if d < 4 else end
+            drain(part(origin, span), ring_recv.at[j, way, d - 1])
+            if d < 4:
+                shifted = AT[sign * (d + 1)] if d < 3 else AT[4]
+                pass_on(origin, shifted, full if d < 3 else end, ahead, ring_recv.at[j, way, d])
+            cross(origin, span)
+        if d == 4 and kind != "g":
+            drain(
+                (rows if kind == "r" else hidden).at[1, :, pl.ds(base, zone), :], ring_pair.at[j]
+            )
+
+    ring_step(0, 0)
+
+    def expert_of(p):
+        to_z = lax.rem(sz - z_step(p) + dim_z, dim_z)
+        return to_z * dim_x + lax.rem(sx - p % dim_x + dim_x, dim_x)
+
+    for z in FAR:
+        base = (z - FAR[0]) * zone
+        far_out[pl.ds(base, zone), :] = jnp.dot(
+            picker[pl.ds(z * zone, zone), :], normed, preferred_element_type=F32
+        ).astype(BF16)
+        for x in range(dim_x):
+            p = z * dim_x + x
+            remote(
+                far_out.at[pl.ds(base + x * block, block), :],
+                rows.at[0, 0, pl.ds(p * block, block), :],
+                small_send.at[5], far_recv.at[z - FAR[0]], sp=expert_of(p),
+            ).start()
+
+    def pick_zone(z, first, last):
+        span = pl.ds(z * zone, zone)
+        wide_rows = jnp.concatenate([norms[k] for k in range(first, last)], axis=1)
+        picked = jnp.dot(picker[span, :], wide_rows, preferred_element_type=F32).astype(BF16)
+        for k in range(first, last):
+            piece = picked[:, (k - first) * 128 : (k - first + 1) * 128]
+            near_out[k, span, :] = piece
+            if z == 0:
+                rows[0, k, pl.ds(0, block), :] = piece[:block]
+        for x in range(dim_x):
+            p = z * dim_x + x
+            if p == 0:
+                continue
             place = pl.ds(p * block, block)
             remote(
-                sent.at[place, :], rows.at[t, place, :], small_send.at[5], disp_recv.at[part],
-                sp=to_z * dim_x + to_x,
+                near_out.at[pl.ds(first, last - first), place, :],
+                rows.at[0, pl.ds(first, last - first), place, :],
+                small_send.at[6], near_recv.at[z], sp=expert_of(p),
             ).start()
+
+    def pick(batch):
+        if batch == 0:
+            for z in EARLY:
+                pick_zone(z, 0, FIRST_SLICES)
+            return
+        for z in EARLY:
+            pick_zone(z, FIRST_SLICES, dim_y)
+        for z in LATE:
+            pick_zone(z, 0, dim_y)
+
+    def across(z):
+        own_x = 1 if z == 0 else 0
+        taken = pl.ds(z * zone, zone - own_x * block)
+        drain(rows.at[0, :, taken, :], near_recv.at[z])
+        span = pl.ds(z * zone, zone)
+        remote(
+            rows.at[0, :, span, :], rows.at[1, :, span, :], small_send.at[8], near_pair.at[z],
+            tp=partner,
+        ).start()
 
     for step_y, other in tp_steps:
         to = at_tp(step_y, other)
@@ -256,90 +366,64 @@
         comb_w[pl.ds(n_rows, n_rows), pl.ds(first, 256)] = (summed - high.astype(F32)).astype(BF16)
         return carry
 
-    def weights(i, part):
+    def weights(z):
         lax.fori_loop(0, slots // 256, fill_weights, 0)
 
-    for load in loads:
-        load.wait()
-
-    lower, upper = chunk // 2, chunk - chunk // 2
-
-    def units(i, part):
-        span = pl.ds(i * chunk + part * lower, lower)
-        held = jnp.concatenate([rows[k, span, :] for k in range(n_tp)], axis=1)
-        both = jnp.dot(held, w_gu[...], preferred_element_type=F32)
+    drain(w_gu.at[:, pl.ds(0, 128)], load_sem.at[0])
+    drain(w_gu.at[:, pl.ds(128, 128)], load_sem.at[1])
+    drain(w_down, load_sem.at[2])
+
+    def stacked_rows(held, z):
+        span = pl.ds(z * zone, zone)
+        return jnp.concatenate(
+            [held[core_no, k, span, :] for core_no in range(2) for k in range(dim_y)], axis=1
+        )
+
+    def units(z):
+        span = pl.ds(z * zone, zone)
+        if z in NEAR:
+            drain(rows.at[1, :, span, :], near_pair.at[z])
+        both = jnp.dot(stacked_rows(rows, z), w_gu[...], preferred_element_type=F32)
         gate = jnp.minimum(both[:, :128], LIMIT)
         up = jnp.clip(both[:, 128:], -LIMIT, LIMIT)
-        hidden[t, span, :] = ((up + 1.0) * (gate * jax.nn.sigmoid(SLOPE * gate))).astype(BF16)
-
-    def outputs(i, part):
-        span = pl.ds(i * chunk + part * lower, lower)
-        held = jnp.concatenate([hidden[k, span, :] for k in range(n_tp)], axis=1)
-        result[span, :] = jnp.dot(held, w_down[...], preferred_element_type=F32).astype(BF16)
-
-    def send_back(i):
-        for p in range(i * per_chunk, (i + 1) * per_chunk):
+        hidden[0, 0, span, :] = ((up + 1.0) * (gate * jax.nn.sigmoid(SLOPE * gate))).astype(BF16)
+
+    def outputs(z):
+        span = pl.ds(z * zone, zone)
+        done = jnp.dot(stacked_rows(hidden, z), w_down[...], preferred_element_type=F32)
+        result[span, :] = done.astype(BF16)
+        for x in range(dim_x):
+            p = z * dim_x + x
             place = pl.ds(p * block, block)
             if p == 0:
                 back[place, :] = result[place, :]
                 continue
             to_z = lax.rem(sz + z_step(p), dim_z)
-            to_x = lax.rem(sx + p % dim_x, dim_x)
+            to_x = lax.rem(sx + x, dim_x)
             remote(
-                result.at[place, :], back.at[place, :], small_send.at[6], back_recv.at[i],
+                result.at[place, :], back.at[place, :], small_send.at[9], back_recv.at[z],
                 sp=to_z * dim_x + to_x,
             ).start()
 
-    right, left = at_tp(1, False), at_tp(-1, False)
-
-    def ring_step(j, d):
-        kind, i = OPS[j]
-        held = rows if kind == "r" else hidden
-        full = pl.ds(i * chunk, chunk)
-        first = pl.ds(i * chunk, lower)
-        second = pl.ds(i * chunk + lower, upper)
-
-        def pass_on(origin, span, to, sem):
-            piece = held.at[origin, span, :]
-            remote(piece, piece, ring_send.at[j], sem, tp=to).start()
-
-        if d == 0:
-            if kind == "r":
-                taken = (per_chunk - (1 if i == 0 else 0)) * block
-                drain(sent.at[pl.ds(0, taken), :], disp_recv.at[i])
-            pass_on(t, full, right, ring_recv.at[j, 0, 0])
-            pass_on(t, full, left, ring_recv.at[j, 1, 0])
-            pass_on(t, full, partner, ring_pair.at[j])
-            return
-        for way, sign, ahead, end in ((0, -1, right, first), (1, 1, left, second)):
-            origin = at_tp(sign * d, False)
-            span = full if d < 4 else end
-            drain(held.at[origin, span, :], ring_recv.at[j, way, d - 1])
-            if d < 4:
-                pass_on(origin, full if d < 3 else end, ahead, ring_recv.at[j, way, d])
-            pass_on(origin, span, partner, ring_pair.at[j])
-        if d == 4:
-            drain(held.at[pl.ds(0, dim_y), full, :], ring_pair.at[j])
-
-    work = {2: [(weights, 0, 0)]}
-    for i in range(CHUNKS):
-        work.setdefault(4 + i, []).extend([(units, i, 0), (units, i, 1)])
-        work.setdefault(9 + i, []).extend([(outputs, i, 0), (outputs, i, 1)])
-    for slot in range(STARTS[-1] + 5):
-        for j in range(len(OPS)):
-            d = slot - STARTS[j]
-            if 0 <= d <= 4:
+    tasks = dict(pick=pick, weights=weights, across=across, units=units)
+    for slot in range(max(op[2] for op in OPS) + 5):
+        finished = []
+        for j, (kind, z, start) in enumerate(OPS):
+            d = slot - start
+            if 0 <= d <= 4 and (j, d) != (0, 0):
                 ring_step(j, d)
-        for task, i, part in work.get(slot, ()):
-            task(i, part)
-            if task is outputs and part == 1:
-                send_back(i)
+                if d == 4 and kind == "h":
+                    finished.append(z)
+        for name, z in WORK.get(slot, ()):
+            tasks[name](z)
+        for z in finished:
+            outputs(z)
 
     summed = jnp.zeros((2 * n_rows, 128), F32)
-    for i in range(CHUNKS):
-        taken = (per_chunk - (1 if i == 0 else 0)) * block
-        drain(back.at[pl.ds(0, taken), :], back_recv.at[i])
-        span = pl.ds(i * chunk, chunk)
+    for z in [op[1] for op in OPS if op[0] == "h"]:
+        taken = zone - (block if z == 0 else 0)
+        drain(back.at[pl.ds(0, taken), :], back_recv.at[z])
+        span = pl.ds(z * zone, zone)
         summed = summed + jnp.dot(comb_w[:, span], back[span, :], preferred_element_type=F32)
     comb_out[...] = (summed[:n_rows] + summed[n_rows:]).astype(BF16)
     for step_y, other in tp_steps:
@@ -351,15 +435,21 @@
     comb_in[t] = comb_out[pl.ds(pl.multiple_of(t * own, own), own), :]
 
     halo.wait_send()
-    drain(w_in.at[pl.ds(0, n_tp - 1)], small_send.at[0])
+    drain(w_in.at[0, pl.ds(0, n_tp - 1)], small_send.at[0])
+    drain(w_in.at[pl.ds(0, dim_x - 1)], small_send.at[10])
     drain(s_in.at[pl.ds(0, n_tp - 1)], small_send.at[1])
     drain(mixed.at[pl.ds(0, 2 * dim_y - 1)], small_send.at[2])
     drain(squares.at[pl.ds(0, n_tp - 1)], small_send.at[3])
     drain(res_in.at[pl.ds(0, n_tp - 1)], small_send.at[4])
-    drain(sent.at[pl.ds(0, slots - block), :], small_send.at[5])
-    drain(result.at[pl.ds(0, slots - block), :], small_send.at[6])
-    for j in range(len(OPS)):
-        drain(rows.at[pl.ds(0, 15), pl.ds(0, chunk), :], ring_send.at[j])
+    drain(far_out, small_send.at[5])
+    drain(near_out.at[:, pl.ds(0, len(NEAR) * zone - block), :], small_send.at[6])
+    drain(near_out, small_send.at[8])
+    drain(result.at[pl.ds(0, slots - block), :], small_send.at[9])
+    for j, op in enumerate(OPS):
+        if op[0] == "g":
+            drain(norms.at[pl.ds(0, 7)], ring_send.at[j])
+        else:
+            drain(rows.at[0, pl.ds(0, 3), pl.ds(0, 5 * zone), :], ring_send.at[j])
 
     drain(res_in.at[pl.ds(0, n_tp - 1)], small_recv.at[3])
     drain(comb_in.at[pl.ds(0, n_tp - 1)], small_recv.at[4])
@@ -382,7 +472,8 @@
     vmem = pl.BlockSpec(memory_space=pltpu.VMEM)
     hbm = pl.BlockSpec(memory_space=pl.ANY)
     dma = pltpu.SemaphoreType.DMA
-    chunks = CHUNKS
+    zone = 4 * n_tp * cap
+    half_tp = n_tp // 2
     return pl.pallas_call(
         functools.partial(kernel, (n_sp, n_tp, 4, cap)),
         out_shape=jax.ShapeDtypeStruct(stream_in.shape, BF16),
@@ -392,7 +483,7 @@
             pltpu.VMEM((16, 128), BF16),
             pltpu.VMEM((16, 128), BF16),
             pltpu.VMEM((n_tp, n_rows // 2, 128), BF16),
-            pltpu.VMEM((n_tp, 64, 128), BF16),
+            pltpu.VMEM((4, n_tp, 16, 128), BF16),
             pltpu.VMEM((n_tp * 128, 256), BF16),
             pltpu.VMEM((n_tp, own, 128), BF16),
             pltpu.VMEM((n_tp, 8, n_rows // 2), F32),
@@ -400,9 +491,11 @@
             pltpu.VMEM((2 * n_rows, slots), BF16),
             pltpu.VMEM((128, n_rows), F32),
             pltpu.VMEM((n_rows, 128), F32),
-            pltpu.VMEM((slots, 128), BF16),
-            pltpu.VMEM((n_tp, slots, 128), BF16),
-            pltpu.VMEM((n_tp, slots, 128), BF16),
+            pltpu.VMEM((half_tp, n_rows, 128), BF16),
+            pltpu.VMEM((len(FAR) * zone, 128), BF16),
+            pltpu.VMEM((half_tp, len(NEAR) * zone, 128), BF16),
+            pltpu.VMEM((2, half_tp, slots, 128), BF16),
+            pltpu.VMEM((2, half_tp, slots, 128), BF16),
             pltpu.VMEM((slots, 128), BF16),
             pltpu.VMEM((slots, 128), BF16),
             pltpu.VMEM((n_rows, 128), BF16),
@@ -411,8 +504,9 @@
             pltpu.VMEM((n_tp, own, 128), BF16),
             pltpu.VMEM((features, 256), BF16),
             pltpu.VMEM((features, 128), BF16),
-            dma((3,)), dma((2,)), dma((8,)), dma((5,)), dma((8,)), dma((chunks,)),
-            dma((len(OPS), 2, 4)), dma((len(OPS),)), dma((len(OPS),)), dma((chunks,)),
+            dma((3,)), dma((2,)), dma((11,)), dma((6,)), dma((8,)), dma((len(FAR),)),
+            dma((len(NEAR),)), dma((len(NEAR),)),
+            dma((len(OPS), 2, 4)), dma((len(OPS),)), dma((len(OPS),)), dma((8,)),
         ],
         compiler_params=pltpu.CompilerParams(
             collective_id=0, has_side_effects=True, vmem_limit_bytes=56 * 1024 * 1024

time: 148 us -> 135 us (0.912)
  Pallas kernels: 146 us -> 133 us
    pallas_call x1, Pallas kernels: 146 us -> 133 us  [local(): pl.pallas_call(functools.partial(kernel, (n_sp, n_tp, 4, cap)), out_shape...]
where the time goes in v3:
time: 135 us
  Pallas kernels  133 us (99%)
  local copies, waits for them, and re-layouts  1.47 us (1%)
    pallas_call x1, Pallas kernels, local(): pl.pallas_call(functools.partial(kernel, (n_sp, n_tp, 4, cap)), out_shape...  133 us

profile of v3, /device:TPU:1, one launch (start us, length us, event | category | flops | bytes accessed | tf_op | source)
XLA Modules:
  0.0 134.9 jit_solution(126275205086736335)
XLA Ops:
  0.0 133.4 %shard_map.127 = bf16[16,2048]{1,0:T(8,128)(2,1)} custom-call(bf16[16,2048]{1,0:T(8,128)(2,1)} %stream.1, bf16[64,256]{1,0:T(8,128)(2,1)} %bitcast.5, bf16[64,256]{1,0:T(8,128)(2,1)} %bitcast.6, bf16[64,256]{1,0:T(8,128)(2,1)} %bitcast.7, bf16[3,64]{1,0:T(4,128)(2,1)} %taps.1, bf16[64,2048]{1,0:T(8,128)(2,1)} %weight.1, s32[4,256]{1,0:T(4,128)} %bitcast.8, ...), custom_call_target="tpu_custom_call" | custom-call | flops 4000000000 | bytes 3000000 | tf_op jit(solution)/shard_map/pallas_call | solution.py:477
  133.4 1.5 %copy.15 = bf16[16,2048]{1,0:T(8,128)(2,1)} copy(bf16[16,2048]{1,0:T(8,128)(2,1)} %shard_map.127) | data formatting | bytes 131072

commit v4 on v3

--- a/solution.py
+++ b/solution.py
@@ -18,15 +18,16 @@
 NEAR, FAR = (0, 1, 2, 3, 4), (5, 6, 7)
 EARLY, LATE = (0, 1, 2), (3, 4)
 FIRST_SLICES = 3
-OPS = (('g', 0, 0), ('r', 5, 2), ('r', 6, 3), ('r', 7, 4), ('h', 5, 7), ('h', 6, 8), ('h', 7, 9), ('h', 0, 10), ('h', 1, 11), ('h', 2, 12), ('h', 3, 13), ('h', 4, 14))
-WORK = {1: [('pick', 0)], 3: [('weights', 0)], 4: [('pick', 1)], 6: [('units', 5)], 7: [('units', 6)], 8: [('units', 7), ('across', 0)], 9: [('units', 0), ('across', 1)], 10: [('units', 1), ('across', 2)], 11: [('units', 2), ('across', 3)], 12: [('units', 3), ('across', 4)], 13: [('units', 4)]}
+OPS = (('g', 0, 0), ('r', 5, 2), ('r', 6, 3), ('r', 7, 4), ('h', 5, 7), ('h', 6, 8), ('h', 7, 9), ('h', 0, 10), ('h', 1, 11), ('h', 2, 12), ('h', 3, 13), ('h', 4, 13))
+WORK = {1: [('pick', 0)], 4: [('pick', 1)], 5: [('pick', 2)], 6: [('pick', 3), ('units', 5)], 7: [('units', 6)], 8: [('units', 7), ('across', 0)], 9: [('units', 0), ('across', 1)], 10: [('units', 1), ('across', 2)], 11: [('units', 2), ('across', 3), ('across', 4)], 12: [('units', 3), ('units', 4)], 13: [('weights', 0), ('weights', 1)], 14: [('weights', 2), ('weights', 3)]}
 
 
 def kernel(
     cfg,
-    stream, pre, value, post, taps, weight, ids, route_w, ffn_gain, post_gain,
-    gate_hbm, up_hbm, down_hbm,
+    stream_hbm, pre_hbm, value_hbm, post_hbm, taps_hbm, weight_hbm, ids_hbm, route_w_hbm,
+    ffn_gain_hbm, post_gain_hbm, gate_hbm, up_hbm, down_hbm,
     out,
+    stream, pre, value, post, taps, weight, ids, route_w, ffn_gain, post_gain, in_sem,
     halo_src, halo_dst, mixed, w_in, w_diag, s_in, squares, picker, comb_w, aux, slot_cols,
     norms, far_out, near_out, rows, hidden, result, back, res_keep, res_in, comb_out, comb_in, w_gu, w_down,
     load_sem, halo_sem, small_send, small_recv, mix_recv, far_recv, near_recv, near_pair,
@@ -64,20 +65,6 @@
         place = p // dim_x
         return (place + 1) // 2 if place % 2 else (dim_z - place // 2) % dim_z
 
-    for core_no in range(2):
-        for place, offset in enumerate(OFFSETS):
-            origin = pl.ds(pl.multiple_of(at_tp(offset, core_no == 1) * 128, 128), 128)
-            here = pl.ds((core_no * dim_y + place) * 128, 128)
-            pltpu.make_async_copy(
-                gate_hbm.at[0, origin, :], w_gu.at[here, pl.ds(0, 128)], load_sem.at[0]
-            ).start()
-            pltpu.make_async_copy(
-                up_hbm.at[0, origin, :], w_gu.at[here, pl.ds(128, 128)], load_sem.at[1]
-            ).start()
-            pltpu.make_async_copy(
-                down_hbm.at[0, origin, :], w_down.at[here, :], load_sem.at[2]
-            ).start()
-
     barrier = pltpu.get_barrier_semaphore()
 
     def greet_tp(step, carry):
@@ -92,13 +79,30 @@
         )
         return carry
 
+    lax.fori_loop(n_sp // 4, n_sp - n_sp // 4, greet_sp, 0)
     lax.fori_loop(1, n_tp, greet_tp, 0)
-    lax.fori_loop(1, n_sp, greet_sp, 0)
+    lax.fori_loop(1, n_sp // 4, greet_sp, 0)
+    lax.fori_loop(n_sp - n_sp // 4, n_sp, greet_sp, 0)
+
+    inputs = [
+        pltpu.make_async_copy(there, here, in_sem.at[k])
+        for k, (there, here) in enumerate((
+            (pre_hbm, pre), (value_hbm, value), (post_hbm, post), (weight_hbm, weight),
+            (taps_hbm, taps), (stream_hbm, stream), (ids_hbm, ids), (route_w_hbm, route_w),
+            (ffn_gain_hbm, ffn_gain), (post_gain_hbm, post_gain),
+        ))
+    ]
+    for copy in inputs:
+        copy.start()
+    for copy in inputs[:3]:
+        copy.wait()
 
     gated = (pre[...].astype(F32) * value[...].astype(F32)).astype(BF16).astype(F32)
     gates = jnp.transpose(jnp.concatenate([gated, post[...].astype(F32)], axis=0))
     halo_src[...] = gates[n_rows - 16 :, :].astype(BF16)
 
+    for copy in inputs[3:]:
+        copy.wait()
     pl.semaphore_wait(barrier, n_tp + n_sp - 2)
 
     halo = remote(
@@ -115,14 +119,37 @@
         remote(
             weight.at[quarter, piece], w_in.at[sx, t], small_send.at[0], small_recv.at[0], tp=to
         ).start()
+    own_cols = pl.ds(pl.multiple_of(t * 128, 128), 128)
+    w_in[sx, t] = weight[quarter, own_cols]
+    s_in[t] = stream[:, own_cols]
+
+    wide, second = gates[:, :channels], gates[:, channels:]
+    tap = taps[...].astype(F32)
+    shift_1, shift_2 = pltpu.roll(wide, 1, 0), pltpu.roll(wide, 2, 0)
+
+    def mixer_rows(two_back, one_back, here, gate):
+        convolved = tap[0:1] * two_back
+        convolved = convolved + tap[1:2] * one_back
+        convolved = convolved + tap[2:3] * here
+        return gate * convolved
+
+    mixer = mixer_rows(shift_2, shift_1, wide, second)
+    body = pl.ds(16, half - 16)
+    head = pl.ds(0, 16)
+    mixed[t, body, :] = jnp.concatenate([mixer[16:half], mixer[half + 16 :]], axis=1).astype(BF16)
+
+    steps = (4, 3, 5, 2, 6, 1, 7)
+    own_body = mixed.at[t, body, :]
+    for step_y in steps:
+        remote(
+            own_body, own_body, small_send.at[2], mix_recv.at[step_y], tp=at_tp(step_y, False)
+        ).start()
+    partner = at_tp(0, True)
+    remote(own_body, own_body, small_send.at[2], mix_recv.at[0], tp=partner).start()
     for step_y, other in tp_steps:
         to = at_tp(step_y, other)
         piece = pl.ds(pl.multiple_of(to * 128, 128), 128)
         remote(stream.at[:, piece], s_in.at[t], small_send.at[1], small_recv.at[1], tp=to).start()
-    own_cols = pl.ds(pl.multiple_of(t * 128, 128), 128)
-    w_in[sx, t] = weight[quarter, own_cols]
-    s_in[t] = stream[:, own_cols]
-
     aux[...] = jnp.zeros_like(aux)
     aux[0:top, :] = ids[...].astype(F32)
     aux[top : 2 * top, :] = route_w[...]
@@ -155,29 +182,34 @@
     slot_rows = jnp.transpose(columns)
     w_diag[...] = jnp.zeros_like(w_diag)
 
-    wide, second = gates[:, :channels], gates[:, channels:]
-    tap = taps[...].astype(F32)
-    row_no = lax.broadcasted_iota(jnp.int32, wide.shape, 0)
-    shift_1, shift_2 = pltpu.roll(wide, 1, 0), pltpu.roll(wide, 2, 0)
+    row_no = lax.broadcasted_iota(jnp.int32, (16, channels), 0)
     halo.wait_recv()
     rim = halo_dst[...].astype(F32)[:, :channels]
     rim = jnp.where(s > 0, rim, 0.0)
     last, before_last = rim[15:16, :], rim[14:15, :]
-    shift_1 = jnp.where(row_no == 0, last, shift_1)
-    shift_2 = jnp.where(row_no == 0, before_last, jnp.where(row_no == 1, last, shift_2))
-    convolved = tap[0:1] * shift_2
-    convolved = convolved + tap[1:2] * shift_1
-    convolved = convolved + tap[2:3] * wide
-    mixer = second * convolved
-    mixed[t] = jnp.concatenate([mixer[:half], mixer[half:]], axis=1).astype(BF16)
-
-    steps = (4, 3, 5, 2, 6, 1, 7)
-    for step_y in steps:
-        remote(
-            mixed.at[t], mixed.at[t], small_send.at[2], mix_recv.at[step_y], tp=at_tp(step_y, False)
-        ).start()
-    partner = at_tp(0, True)
-    remote(mixed.at[t], mixed.at[t], small_send.at[2], mix_recv.at[0], tp=partner).start()
+    one_back = jnp.where(row_no == 0, last, shift_1[:16])
+    two_back = jnp.where(row_no == 0, before_last, jnp.where(row_no == 1, last, shift_2[:16]))
+    first_rows = mixer_rows(two_back, one_back, wide[:16], second[:16])
+    mixed[t, head, :] = jnp.concatenate([first_rows, mixer[half : half + 16]], axis=1).astype(BF16)
+    own_head = mixed.at[t, head, :]
+    for step_y, other in tp_steps:
+        remote(
+            own_head, own_head, small_send.at[11], small_recv.at[6], tp=at_tp(step_y, other)
+        ).start()
+    for core_no in range(2):
+        for place, offset in enumerate(OFFSETS):
+            origin = pl.ds(pl.multiple_of(at_tp(offset, core_no == 1) * 128, 128), 128)
+            here = pl.ds((core_no * dim_y + place) * 128, 128)
+            pltpu.make_async_copy(
+                gate_hbm.at[0, origin, :], w_gu.at[here, pl.ds(0, 128)], load_sem.at[0]
+            ).start()
+            pltpu.make_async_copy(
+                up_hbm.at[0, origin, :], w_gu.at[here, pl.ds(128, 128)], load_sem.at[1]
+            ).start()
+            pltpu.make_async_copy(
+                down_hbm.at[0, origin, :], w_down.at[here, :], load_sem.at[2]
+            ).start()
+
     drain(w_in.at[sx, pl.ds(0, n_tp - 1)], small_recv.at[0])
     for step_x in (2, 1, 3):
         remote(
@@ -203,11 +235,12 @@
         w_diag[pl.ds(k * 128, 64), pl.ds(0, 128)] = piece
         w_diag[pl.ds(k * 128 + 64, 64), pl.ds(128, 128)] = piece
     for step_y in steps:
-        arrived = mixed.at[at_tp(-step_y, False)]
+        arrived = mixed.at[at_tp(-step_y, False), body, :]
         drain(arrived, mix_recv.at[step_y])
         remote(arrived, arrived, small_send.at[2], mix_recv.at[0], tp=partner).start()
     drain(s_in.at[pl.ds(0, n_tp - 1)], small_recv.at[1])
-    drain(mixed.at[pl.ds(0, dim_y)], mix_recv.at[0])
+    drain(mixed.at[pl.ds(0, dim_y), body, :], mix_recv.at[0])
+    drain(mixed.at[pl.ds(0, n_tp - 1), head, :], small_recv.at[6])
     stacked = jnp.concatenate([mixed[k] for k in range(n_tp)], axis=1)
     projected = jnp.dot(stacked, w_diag[...], preferred_element_type=F32)
     projected = jnp.concatenate([projected[:, :128], projected[:, 128:]], axis=0)
@@ -328,10 +361,11 @@
             for z in EARLY:
                 pick_zone(z, 0, FIRST_SLICES)
             return
-        for z in EARLY:
-            pick_zone(z, FIRST_SLICES, dim_y)
-        for z in LATE:
-            pick_zone(z, 0, dim_y)
+        if batch == 1:
+            for z in EARLY:
+                pick_zone(z, FIRST_SLICES, dim_y)
+            return
+        pick_zone(LATE[batch - 2], 0, dim_y)
 
     def across(z):
         own_x = 1 if z == 0 else 0
@@ -367,7 +401,7 @@
         return carry
 
     def weights(z):
-        lax.fori_loop(0, slots // 256, fill_weights, 0)
+        lax.fori_loop(z * (slots // 1024), (z + 1) * (slots // 1024), fill_weights, 0)
 
     drain(w_gu.at[:, pl.ds(0, 128)], load_sem.at[0])
     drain(w_gu.at[:, pl.ds(128, 128)], load_sem.at[1])
@@ -408,7 +442,7 @@
     tasks = dict(pick=pick, weights=weights, across=across, units=units)
     for slot in range(max(op[2] for op in OPS) + 5):
         finished = []
-        for j, (kind, z, start) in enumerate(OPS):
+        for j, (kind, z, start) in reversed(list(enumerate(OPS))):
             d = slot - start
             if 0 <= d <= 4 and (j, d) != (0, 0):
                 ring_step(j, d)
@@ -438,7 +472,8 @@
     drain(w_in.at[0, pl.ds(0, n_tp - 1)], small_send.at[0])
     drain(w_in.at[pl.ds(0, dim_x - 1)], small_send.at[10])
     drain(s_in.at[pl.ds(0, n_tp - 1)], small_send.at[1])
-    drain(mixed.at[pl.ds(0, 2 * dim_y - 1)], small_send.at[2])
+    drain(mixed.at[pl.ds(0, 2 * dim_y - 1), body, :], small_send.at[2])
+    drain(mixed.at[pl.ds(0, n_tp - 1), head, :], small_send.at[11])
     drain(squares.at[pl.ds(0, n_tp - 1)], small_send.at[3])
     drain(res_in.at[pl.ds(0, n_tp - 1)], small_send.at[4])
     drain(far_out, small_send.at[5])
@@ -477,9 +512,20 @@
     return pl.pallas_call(
         functools.partial(kernel, (n_sp, n_tp, 4, cap)),
         out_shape=jax.ShapeDtypeStruct(stream_in.shape, BF16),
-        in_specs=[vmem] * 10 + [hbm] * 3,
+        in_specs=[hbm] * 13,
         out_specs=vmem,
         scratch_shapes=[
+            pltpu.VMEM(stream_in.shape, BF16),
+            pltpu.VMEM(pre_gate.shape[::-1], BF16),
+            pltpu.VMEM(pre_gate.shape[::-1], BF16),
+            pltpu.VMEM(pre_gate.shape[::-1], BF16),
+            pltpu.VMEM(conv_taps.shape, BF16),
+            pltpu.VMEM(out_weight.shape, BF16),
+            pltpu.VMEM(route_ids.shape[::-1], jnp.int32),
+            pltpu.VMEM(route_weight.shape[::-1], F32),
+            pltpu.VMEM(ffn_gain.shape, BF16),
+            pltpu.VMEM(post_gain.shape, BF16),
+            dma((10,)),
             pltpu.VMEM((16, 128), BF16),
             pltpu.VMEM((16, 128), BF16),
             pltpu.VMEM((n_tp, n_rows // 2, 128), BF16),
@@ -504,12 +550,12 @@
             pltpu.VMEM((n_tp, own, 128), BF16),
             pltpu.VMEM((features, 256), BF16),
             pltpu.VMEM((features, 128), BF16),
-            dma((3,)), dma((2,)), dma((11,)), dma((6,)), dma((8,)), dma((len(FAR),)),
+            dma((3,)), dma((2,)), dma((12,)), dma((7,)), dma((8,)), dma((len(FAR),)),
             dma((len(NEAR),)), dma((len(NEAR),)),
             dma((len(OPS), 2, 4)), dma((len(OPS),)), dma((len(OPS),)), dma((8,)),
         ],
         compiler_params=pltpu.CompilerParams(
-            collective_id=0, has_side_effects=True, vmem_limit_bytes=56 * 1024 * 1024
+            collective_id=0, has_side_effects=True, vmem_limit_bytes=63 * 1024 * 1024
         ),
         cost_estimate=pl.CostEstimate(flops=4 * 10**9, bytes_accessed=3 * 10**6, transcendentals=0),
     )(

time: 135 us -> 130 us (0.963)
  Pallas kernels: 133 us -> 128 us
    pallas_call x1, Pallas kernels: 133 us -> 128 us  [local(): pl.pallas_call(functools.partial(kernel, (n_sp, n_tp, 4, cap)), out_shape...]
where the time goes in v4:
time: 130 us
  Pallas kernels  128 us (98%)
  local copies, waits for them, and re-layouts  1.47 us (1%)
    pallas_call x1, Pallas kernels, local(): pl.pallas_call(functools.partial(kernel, (n_sp, n_tp, 4, cap)), out_shape...  128 us

profile of v4, /device:TPU:1, one launch (start us, length us, event | category | flops | bytes accessed | tf_op | source)
XLA Modules:
  0.0 129.6 jit_solution(4193281211748140764)
XLA Ops:
  0.0 128.1 %shard_map.127 = bf16[16,2048]{1,0:T(8,128)(2,1)} custom-call(bf16[16,2048]{1,0:T(8,128)(2,1)} %stream_hbm.1, bf16[64,256]{1,0:T(8,128)(2,1)} %bitcast.5, bf16[64,256]{1,0:T(8,128)(2,1)} %bitcast.6, bf16[64,256]{1,0:T(8,128)(2,1)} %bitcast.7, bf16[3,64]{1,0:T(4,128)(2,1)} %taps_hbm.1, bf16[64,2048]{1,0:T(8,128)(2,1)} %weight_hbm.1, s32[4,256]{1,0:T(4,128)} %bitcast.8, ...), custom_call_target="tpu_custom_call" | custom-call | flops 4000000000 | bytes 3000000 | tf_op jit(solution)/shard_map/pallas_call | solution.py:512
  128.1 1.5 %copy.15 = bf16[16,2048]{1,0:T(8,128)(2,1)} copy(bf16[16,2048]{1,0:T(8,128)(2,1)} %shard_map.127) | data formatting | bytes 131072

commit v5 on v4

--- a/solution.py
+++ b/solution.py
@@ -18,8 +18,8 @@
 NEAR, FAR = (0, 1, 2, 3, 4), (5, 6, 7)
 EARLY, LATE = (0, 1, 2), (3, 4)
 FIRST_SLICES = 3
-OPS = (('g', 0, 0), ('r', 5, 2), ('r', 6, 3), ('r', 7, 4), ('h', 5, 7), ('h', 6, 8), ('h', 7, 9), ('h', 0, 10), ('h', 1, 11), ('h', 2, 12), ('h', 3, 13), ('h', 4, 13))
-WORK = {1: [('pick', 0)], 4: [('pick', 1)], 5: [('pick', 2)], 6: [('pick', 3), ('units', 5)], 7: [('units', 6)], 8: [('units', 7), ('across', 0)], 9: [('units', 0), ('across', 1)], 10: [('units', 1), ('across', 2)], 11: [('units', 2), ('across', 3), ('across', 4)], 12: [('units', 3), ('units', 4)], 13: [('weights', 0), ('weights', 1)], 14: [('weights', 2), ('weights', 3)]}
+OPS = (('g', 0, 0), ('r', 5, 2), ('r', 6, 3), ('r', 7, 6), ('h', 5, 7), ('h', 6, 8), ('h', 0, 9), ('h', 1, 10), ('h', 7, 11), ('h', 2, 12), ('h', 3, 13), ('h', 4, 13))
+WORK = {1: [('pick', 0)], 4: [('pick', 1)], 5: [('pick', 2)], 6: [('pick', 3), ('units', 5)], 13: [('weights', 0), ('weights', 1)], 14: [('weights', 2), ('weights', 3)], 7: [('units', 6), ('across', 0)], 8: [('units', 0), ('across', 1)], 9: [('units', 1)], 10: [('units', 7), ('across', 2)], 11: [('units', 2), ('across', 3), ('across', 4)], 12: [('units', 3), ('units', 4)]}
 
 
 def kernel(

time: 130 us -> 127 us (0.977)
  Pallas kernels: 128 us -> 126 us
    pallas_call x1, Pallas kernels: 128 us -> 126 us  [local(): pl.pallas_call(functools.partial(kernel, (n_sp, n_tp, 4, cap)), out_shape...]
where the time goes in v5:
time: 127 us
  Pallas kernels  126 us (99%)
  local copies, waits for them, and re-layouts  1.47 us (1%)
    pallas_call x1, Pallas kernels, local(): pl.pallas_call(functools.partial(kernel, (n_sp, n_tp, 4, cap)), out_shape...  126 us

profile of v5, /device:TPU:1, one launch (start us, length us, event | category | flops | bytes accessed | tf_op | source)
XLA Modules:
  0.0 127.2 jit_solution(2163231590806972964)
XLA Ops:
  0.0 125.7 %shard_map.127 = bf16[16,2048]{1,0:T(8,128)(2,1)} custom-call(bf16[16,2048]{1,0:T(8,128)(2,1)} %stream_hbm.1, bf16[64,256]{1,0:T(8,128)(2,1)} %bitcast.5, bf16[64,256]{1,0:T(8,128)(2,1)} %bitcast.6, bf16[64,256]{1,0:T(8,128)(2,1)} %bitcast.7, bf16[3,64]{1,0:T(4,128)(2,1)} %taps_hbm.1, bf16[64,2048]{1,0:T(8,128)(2,1)} %weight_hbm.1, s32[4,256]{1,0:T(4,128)} %bitcast.8, ...), custom_call_target="tpu_custom_call" | custom-call | flops 4000000000 | bytes 3000000 | tf_op jit(solution)/shard_map/pallas_call | solution.py:512
  125.7 1.5 %copy.15 = bf16[16,2048]{1,0:T(8,128)(2,1)} copy(bf16[16,2048]{1,0:T(8,128)(2,1)} %shard_map.127) | data formatting | bytes 131072

commit v6 on v5

--- a/solution.py
+++ b/solution.py
@@ -440,14 +440,18 @@
             ).start()
 
     tasks = dict(pick=pick, weights=weights, across=across, units=units)
-    for slot in range(max(op[2] for op in OPS) + 5):
+    last_slot = max(op[2] for op in OPS) + 4
+    for slot in range(last_slot + 1):
         finished = []
         for j, (kind, z, start) in reversed(list(enumerate(OPS))):
             d = slot - start
             if 0 <= d <= 4 and (j, d) != (0, 0):
                 ring_step(j, d)
                 if d == 4 and kind == "h":
-                    finished.append(z)
+                    if slot == last_slot:
+                        outputs(z)
+                    else:
+                        finished.append(z)
         for name, z in WORK.get(slot, ()):
             tasks[name](z)
         for z in finished:

time: 127 us -> 127 us (level)
  no operation moved by 1% of the time
where the time goes in v6:
time: 127 us
  Pallas kernels  126 us (99%)
  local copies, waits for them, and re-layouts  1.47 us (1%)
    pallas_call x1, Pallas kernels, local(): pl.pallas_call(functools.partial(kernel, (n_sp, n_tp, 4, cap)), out_shape...  126 us

profile of v6, /device:TPU:1, one launch (start us, length us, event | category | flops | bytes accessed | tf_op | source)
XLA Modules:
  0.0 127.1 jit_solution(15777028276269783546)
XLA Ops:
  0.0 125.6 %shard_map.127 = bf16[16,2048]{1,0:T(8,128)(2,1)} custom-call(bf16[16,2048]{1,0:T(8,128)(2,1)} %stream_hbm.1, bf16[64,256]{1,0:T(8,128)(2,1)} %bitcast.5, bf16[64,256]{1,0:T(8,128)(2,1)} %bitcast.6, bf16[64,256]{1,0:T(8,128)(2,1)} %bitcast.7, bf16[3,64]{1,0:T(4,128)(2,1)} %taps_hbm.1, bf16[64,2048]{1,0:T(8,128)(2,1)} %weight_hbm.1, s32[4,256]{1,0:T(4,128)} %bitcast.8, ...), custom_call_target="tpu_custom_call" | custom-call | flops 4000000000 | bytes 3000000 | tf_op jit(solution)/shard_map/pallas_call | solution.py:516
  125.6 1.5 %copy.15 = bf16[16,2048]{1,0:T(8,128)(2,1)} copy(bf16[16,2048]{1,0:T(8,128)(2,1)} %shard_map.127) | data formatting | bytes 131072
